TPU v7x, 32 devices: a whole 2x2x4 slice. The times are simulated.
32 devices in a mesh: sp: 8 (over z, y), tp: 4 (over x, core).
Axes of the slice: x: 2, y: 2, z: 4, core: 2. Of those that a mesh axis runs over, the one named last changes fastest.
Arguments:
- resid_in: bfloat16 [3072, 2048], P('sp'), may hold values from -6 to 6
- cotangent: bfloat16 [3072, 2048], P('sp'), may hold values from -2 to 2
- norm_gain: float32 [2048], replicated, may hold values from 0.1 to 1.9
- routes: int32 [3072, 2], P('sp'), may hold values from 0 to 7, all different within a row; in each aligned block of 384 rows (0 to 383, 384 to 767, ...) at most 192 rows name the same one
- route_weights: float32 [3072, 2], P('sp'), may hold values from 0.1 to 1
- gate_weight: bfloat16 [8, 2048, 1024], P('sp', None, 'tp'), may hold values from -0.125 to 0.125
- up_weight: bfloat16 [8, 2048, 1024], P('sp', None, 'tp'), may hold values from -0.125 to 0.125
- down_weight: bfloat16 [8, 1024, 2048], P('sp', 'tp'), may hold values from -0.1875 to 0.1875
- out_weight: bfloat16 [2048, 1024], P(None, 'tp'), may hold values from -0.1875 to 0.1875
- gate_b: bfloat16 [3072, 1024], P('sp', 'tp'), may hold values from -6 to 6
- gate_c: bfloat16 [3072, 1024], P('sp', 'tp'), may hold values from -6 to 6
- values_u: bfloat16 [3072, 1024], P('sp', 'tp'), may hold values from -6 to 6
- taps: float32 [3, 1024], P(None, 'tp'), may hold values from -3.5 to 3.5
Outputs:
- grad_gate_weight: float32 [8, 2048, 1024], P('sp', None, 'tp')
- grad_up_weight: float32 [8, 2048, 1024], P('sp', None, 'tp')
- grad_down_weight: float32 [8, 1024, 2048], P('sp', 'tp')
- grad_resid: bfloat16 [3072, 2048], P('sp')
- grad_out_weight: float32 [2048, 1024], P('sp', 'tp')
- grad_gate_b: bfloat16 [3072, 1024], P('sp', 'tp')
- grad_gate_c: bfloat16 [3072, 1024], P('sp', 'tp')
- grad_values: bfloat16 [3072, 1024], P('sp', 'tp')
Inputs may be any that keep to these rules, and one draw needn't show every extreme that they name: `routes`: A row's 2 experts differ. In the rows of one index of sp (384 tokens) no expert is named more than 192 times, a bound that some block reaches.
All inputs are finite; a program needn't handle non-finite values.
Results may differ from a plain program's by a relative error of at most 0.024.
Values may be sent and summed in bfloat16 or wider, within the bound.
A program may use at most 128 MiB of HBM per device.

v0:
```python
import functools

import jax
import jax.numpy as jnp
from jax import lax
from jax.experimental import pallas as pl
from jax.experimental.pallas import tpu as pltpu
from jax.sharding import PartitionSpec as P

norm_eps = 1e-06


def passed_along(array, axis, by):
    size = lax.axis_size(axis)
    pairs = [(i, i + by) for i in range(size) if 0 <= i + by < size]
    return lax.ppermute(array, axis, pairs)


def remote(source, target, send_sem, recv_sem, **device):
    return pltpu.make_async_remote_copy(
        src_ref=source,
        dst_ref=target,
        send_sem=send_sem,
        recv_sem=recv_sem,
        device_id=device,
        device_id_type=pl.DeviceIdType.MESH,
    )


def greet(groups, spot, core_peer, far_peer):
    barrier = pltpu.get_barrier_semaphore()

    def to_group(offset, carry):
        pl.semaphore_signal(
            barrier,
            inc=1,
            device_id={"sp": lax.rem(spot + offset, groups)},
            device_id_type=pl.DeviceIdType.MESH,
        )
        return carry

    lax.fori_loop(1, groups, to_group, 0)
    for peer in (core_peer, far_peer):
        pl.semaphore_signal(
            barrier, inc=1, device_id={"tp": peer}, device_id_type=pl.DeviceIdType.MESH
        )
    pl.semaphore_wait(barrier, groups + 1)


def dispatch_kernel(
    groups,
    lanes,
    sent_rows,
    sent_cots,
    sent_weights,
    got_rows,
    got_cots,
    got_weights,
    local_sem,
    send_a,
    recv_a,
    send_x,
    recv_x,
    send_c,
    recv_c,
    send_f,
    recv_f,
    send_w,
    recv_w,
):
    spot, lane = lax.axis_index("sp"), lax.axis_index("tp")
    core_peer = lane + 1 - 2 * lax.rem(lane, 2)
    far_peer = lax.rem(lane + lanes // 2, lanes)
    quarter = sent_rows.shape[2]
    pairs = ((sent_rows, got_rows), (sent_cots, got_cots))

    def part(ref, block, who):
        return ref.at[block, :, pl.ds(pl.multiple_of(who * quarter, quarter), quarter)]

    def across(k, offset):
        goal = lax.rem(spot + offset, groups)
        return remote(
            pairs[k][0].at[goal],
            part(pairs[k][1], spot, lane),
            send_a.at[k, offset],
            recv_a.at[k, offset],
            sp=goal,
        )

    def weights_across(offset):
        goal = lax.rem(spot + offset, groups)
        return remote(
            sent_weights.at[goal],
            got_weights.at[spot],
            send_w.at[offset],
            recv_w.at[offset],
            sp=goal,
        )

    def origin(offset):
        return lax.rem(spot - offset + groups, groups)

    def sideways(k, offset, source, far):
        sems = (send_x, recv_x) if far else (send_c, recv_c)
        return remote(
            source,
            part(pairs[k][1], origin(offset), lane),
            sems[0].at[k, offset],
            sems[1].at[k, offset],
            tp=far_peer if far else core_peer,
        )

    def forward(k, offset):
        held = part(pairs[k][1], origin(offset), far_peer)
        return remote(held, held, send_f.at[k, offset], recv_f.at[k, offset], tp=core_peer)

    greet(groups, spot, core_peer, far_peer)
    own = [
        pltpu.make_async_copy(
            pairs[k][0].at[spot], part(pairs[k][1], spot, lane), local_sem.at[k]
        )
        for k in (0, 1)
    ]
    own_weights = pltpu.make_async_copy(
        sent_weights.at[spot], got_weights.at[spot], local_sem.at[2]
    )

    def launch(offset, carry):
        weights_across(offset).start()
        for k in (0, 1):
            across(k, offset).start()
        return carry

    lax.fori_loop(1, groups, launch, 0)
    for k in (0, 1):
        for far in (True, False):
            sideways(k, 0, pairs[k][0].at[spot], far).start()
    for copy in own:
        copy.start()
    own_weights.start()

    def pass_on(offset, carry):
        for k in (0, 1):
            across(k, offset).wait_recv()
            for far in (True, False):
                sideways(k, offset, part(pairs[k][1], origin(offset), lane), far).start()
        for k in (0, 1):
            sideways(k, offset - 1, part(pairs[k][1], origin(offset - 1), lane), True).wait_recv()
            forward(k, offset - 1).start()
        return carry

    lax.fori_loop(1, groups, pass_on, 0)
    for k in (0, 1):
        last = groups - 1
        sideways(k, last, part(pairs[k][1], origin(last), lane), True).wait_recv()
        forward(k, last).start()

    def finish(offset, carry):
        for k in (0, 1):
            mine = part(pairs[k][1], origin(offset), lane)
            sideways(k, offset, mine, True).wait_send()
            sideways(k, offset, mine, False).wait()
            forward(k, offset).wait()
        return carry

    def finish_across(offset, carry):
        weights_across(offset).wait()
        for k in (0, 1):
            across(k, offset).wait_send()
        return carry

    lax.fori_loop(0, groups, finish, 0)
    lax.fori_loop(1, groups, finish_across, 0)
    for copy in own:
        copy.wait()
    own_weights.wait()


def dispatch(sent_rows, sent_cots, sent_weights, groups, lanes):
    span, quarter = sent_rows.shape[1:]
    whole = jax.ShapeDtypeStruct((groups, span, quarter * lanes), sent_rows.dtype)
    sem = pltpu.SemaphoreType.DMA
    anywhere = pl.BlockSpec(memory_space=pl.ANY)
    wire = 2 * span * quarter * 2 * groups * 3
    return pl.pallas_call(
        functools.partial(dispatch_kernel, groups, lanes),
        out_shape=(
            whole,
            whole,
            jax.ShapeDtypeStruct(sent_weights.shape, sent_weights.dtype),
        ),
        in_specs=[anywhere] * 3,
        out_specs=(anywhere,) * 3,
        scratch_shapes=[sem((3,))] + [sem((2, groups))] * 8 + [sem((groups,))] * 2,
        compiler_params=pltpu.CompilerParams(collective_id=1, has_side_effects=True),
        cost_estimate=pl.CostEstimate(
            flops=0, bytes_accessed=40 * wire, transcendentals=0
        ),
        name="dispatch",
    )(sent_rows, sent_cots, sent_weights)


def collect_kernel(
    groups,
    lanes,
    partial,
    returned,
    from_core,
    to_far,
    from_far,
    summed,
    send_c,
    recv_c,
    send_x,
    recv_x,
    send_a,
    recv_a,
):
    f32 = jnp.float32
    bf16 = jnp.bfloat16
    spot, lane = lax.axis_index("sp"), lax.axis_index("tp")
    core_peer = lane + 1 - 2 * lax.rem(lane, 2)
    far_peer = lax.rem(lane + lanes // 2, lanes)
    quarter = returned.shape[2]

    def part(block, who):
        return partial.at[block, :, pl.ds(pl.multiple_of(who * quarter, quarter), quarter)]

    def goal_of(step):
        return lax.rem(spot + step + 1, groups)

    def to_core(step, far):
        who = lax.rem(core_peer + far * (lanes // 2), lanes)
        return remote(
            part(goal_of(step), who),
            from_core.at[step, far],
            send_c.at[step, far],
            recv_c.at[step, far],
            tp=core_peer,
        )

    def to_far_peer(step):
        return remote(
            to_far.at[step], from_far.at[step], send_x.at[step], recv_x.at[step], tp=far_peer
        )

    def home(step):
        goal = goal_of(step)
        return remote(
            summed.at[step], returned.at[spot], send_a.at[step], recv_a.at[step], sp=goal
        )

    greet(groups, spot, core_peer, far_peer)

    def begin(step, carry):
        to_core(step, 1).start()
        to_core(step, 0).start()
        return carry

    lax.fori_loop(0, groups, begin, 0)

    def middle(step, carry):
        to_core(step, 1).wait_recv()
        to_far[step] = (
            part(goal_of(step), far_peer)[...].astype(f32) + from_core[step, 1].astype(f32)
        ).astype(bf16)
        to_far_peer(step).start()
        return carry

    lax.fori_loop(0, groups, middle, 0)

    def total(step):
        to_core(step, 0).wait_recv()
        to_far_peer(step).wait_recv()
        return (
            part(goal_of(step), lane)[...].astype(f32)
            + from_core[step, 0].astype(f32)
            + from_far[step].astype(f32)
        ).astype(bf16)

    def end(step, carry):
        summed[step] = total(step)
        home(step).start()
        return carry

    lax.fori_loop(0, groups - 1, end, 0)
    returned[spot] = total(groups - 1)

    def finish(step, carry):
        to_core(step, 0).wait_send()
        to_core(step, 1).wait_send()
        to_far_peer(step).wait_send()
        return carry

    lax.fori_loop(0, groups, finish, 0)

    def finish_home(step, carry):
        home(step).wait()
        return carry

    lax.fori_loop(0, groups - 1, finish_home, 0)


def collect(partial, groups, lanes):
    span, width = partial.shape[1:]
    quarter = width // lanes
    block = (groups, span, quarter)
    sem = pltpu.SemaphoreType.DMA
    inside = pl.BlockSpec(memory_space=pltpu.VMEM)
    return pl.pallas_call(
        functools.partial(collect_kernel, groups, lanes),
        out_shape=jax.ShapeDtypeStruct(block, partial.dtype),
        in_specs=[inside],
        out_specs=inside,
        scratch_shapes=[
            pltpu.VMEM((groups, 2, span, quarter), partial.dtype),
            pltpu.VMEM(block, partial.dtype),
            pltpu.VMEM(block, partial.dtype),
            pltpu.VMEM(block, partial.dtype),
            sem((groups, 2)),
            sem((groups, 2)),
        ]
        + [sem((groups,))] * 4,
        compiler_params=pltpu.CompilerParams(
            collective_id=2, has_side_effects=True, vmem_limit_bytes=40 * 2**20
        ),
        cost_estimate=pl.CostEstimate(
            flops=0, bytes_accessed=150 * 2**20, transcendentals=0
        ),
        name="collect",
    )(partial)


def gather_kernel(groups, lanes, mine, gathered, own_sem, send_sems, recv_sems):
    spot, lane = lax.axis_index("sp"), lax.axis_index("tp")
    core_peer = lane + 1 - 2 * lax.rem(lane, 2)
    far_peer = lax.rem(lane + lanes // 2, lanes)
    quarter = mine.shape[1]

    def part(who):
        return gathered.at[:, pl.ds(pl.multiple_of(who * quarter, quarter), quarter)]

    greet(groups, spot, core_peer, far_peer)
    far = remote(mine, part(lane), send_sems.at[0], recv_sems.at[0], tp=far_peer)
    near = remote(mine, part(lane), send_sems.at[1], recv_sems.at[1], tp=core_peer)
    own = pltpu.make_async_copy(mine, part(lane), own_sem)
    far.start()
    near.start()
    own.start()
    far.wait_recv()
    passed = remote(
        part(far_peer), part(far_peer), send_sems.at[2], recv_sems.at[2], tp=core_peer
    )
    passed.start()
    far.wait_send()
    near.wait()
    own.wait()
    passed.wait()


def gather_quarters(mine, groups, lanes):
    sem = pltpu.SemaphoreType.DMA
    inside = pl.BlockSpec(memory_space=pltpu.VMEM)
    return pl.pallas_call(
        functools.partial(gather_kernel, groups, lanes),
        out_shape=jax.ShapeDtypeStruct((mine.shape[0], mine.shape[1] * lanes), mine.dtype),
        in_specs=[inside],
        out_specs=inside,
        scratch_shapes=[sem, sem((3,)), sem((3,))],
        compiler_params=pltpu.CompilerParams(collective_id=3, has_side_effects=True),
        name="gather_quarters",
    )(mine)


def reduce_kernel(groups, lanes, partial, total, arrived, send_sems, recv_sems):
    f32 = jnp.float32
    spot, lane = lax.axis_index("sp"), lax.axis_index("tp")
    core_peer = lane + 1 - 2 * lax.rem(lane, 2)
    far_peer = lax.rem(lane + lanes // 2, lanes)

    def across(offset):
        goal = lax.rem(spot + offset, groups)
        return remote(
            partial.at[goal],
            arrived.at[offset],
            send_sems.at[offset],
            recv_sems.at[offset],
            sp=goal,
        )

    greet(groups, spot, core_peer, far_peer)

    def launch(offset, carry):
        across(offset).start()
        return carry

    lax.fori_loop(1, groups, launch, 0)
    total[...] = partial[spot].astype(f32)

    def add(offset, carry):
        across(offset).wait_recv()
        total[...] += arrived[offset].astype(f32)
        return carry

    lax.fori_loop(1, groups, add, 0)

    def finish(offset, carry):
        across(offset).wait_send()
        return carry

    lax.fori_loop(1, groups, finish, 0)


def reduce_rows(partial, groups, lanes):
    sem = pltpu.SemaphoreType.DMA
    inside = pl.BlockSpec(memory_space=pltpu.VMEM)
    return pl.pallas_call(
        functools.partial(reduce_kernel, groups, lanes),
        out_shape=jax.ShapeDtypeStruct(partial.shape[1:], jnp.float32),
        in_specs=[inside],
        out_specs=inside,
        scratch_shapes=[
            pltpu.VMEM(partial.shape, partial.dtype),
            sem((groups,)),
            sem((groups,)),
        ],
        compiler_params=pltpu.CompilerParams(collective_id=4, has_side_effects=True),
        name="reduce_rows",
    )(partial)


def expert_pass(entry_rows, entry_cots, entry_weights, gate_mat, up_mat, down_mat):
    f32 = jnp.float32
    bf16 = jnp.bfloat16
    gate_pre = jnp.dot(entry_rows, gate_mat, preferred_element_type=f32)
    up_pre = jnp.dot(entry_rows, up_mat, preferred_element_type=f32)
    logistic = jax.nn.sigmoid(gate_pre)
    activated = gate_pre * logistic
    hidden = (activated * up_pre * entry_weights[:, None]).astype(bf16)
    grad_down = jnp.einsum("rf,rd->fd", hidden, entry_cots, preferred_element_type=f32)
    dhidden = (
        jnp.einsum("rd,fd->rf", entry_cots, down_mat, preferred_element_type=f32)
        * entry_weights[:, None]
    )
    dgate = (dhidden * up_pre * logistic * (1.0 + gate_pre * (1.0 - logistic))).astype(bf16)
    dup = (dhidden * activated).astype(bf16)
    grad_gate = jnp.einsum("rd,rf->df", entry_rows, dgate, preferred_element_type=f32)
    grad_up = jnp.einsum("rd,rf->df", entry_rows, dup, preferred_element_type=f32)
    partial_sum = jnp.einsum("rf,df->rd", dgate, gate_mat, preferred_element_type=f32) + jnp.einsum(
        "rf,df->rd", dup, up_mat, preferred_element_type=f32
    )
    return (grad_gate, grad_up, grad_down, partial_sum)


def on_device(
    resid_in,
    cotangent,
    norm_gain,
    routes,
    route_weights,
    gate_weight,
    up_weight,
    down_weight,
    out_weight,
    gate_b,
    gate_c,
    values_u,
    taps,
):
    f32 = jnp.float32
    bf16 = jnp.bfloat16
    token_count, model_width = resid_in.shape
    groups = lax.axis_size("sp")
    lanes = lax.axis_size("tp")
    local_experts = gate_weight.shape[0]
    expert_total = local_experts * groups
    capacity = 4 * token_count // expert_total
    slot_span = local_experts * capacity
    resid_wide = resid_in.astype(f32)
    inv_rms = lax.rsqrt(jnp.mean(resid_wide * resid_wide, axis=1, keepdims=True) + norm_eps)
    normed = (resid_wide * inv_rms * norm_gain).astype(bf16)
    mixed = gate_c.astype(f32) * values_u.astype(f32)
    earlier = passed_along(mixed[-2:], "sp", 1)
    quarter = model_width // lanes
    lane = lax.axis_index("tp")
    slots = expert_total * capacity
    names = jnp.arange(expert_total, dtype=jnp.int32)
    chosen = routes[:, :, None] == names[None, None, :]
    named = jnp.any(chosen, axis=1).astype(bf16)
    order = jnp.arange(token_count, dtype=jnp.int32)
    strict = (order[:, None] > order[None, :]).astype(bf16)
    before = jnp.dot(strict, named, preferred_element_type=f32).astype(jnp.int32)
    rank = jnp.sum(jnp.where(chosen, before[:, None, :], 0), axis=2)
    targets = routes * capacity + rank
    slot_ids = jnp.arange(slots, dtype=jnp.int32)[:, None]
    first = slot_ids == targets[:, 0][None, :]
    second = slot_ids == targets[:, 1][None, :]
    placing = (first | second).astype(bf16)
    sent_weights = jnp.sum(
        jnp.where(first, route_weights[:, 0][None, :], 0.0)
        + jnp.where(second, route_weights[:, 1][None, :], 0.0),
        axis=1,
    ).reshape(groups, slot_span)
    own_rows = lax.dynamic_slice_in_dim(normed, lane * quarter, quarter, axis=1)
    own_cots = lax.dynamic_slice_in_dim(cotangent, lane * quarter, quarter, axis=1)
    sent_rows = jnp.dot(placing, own_rows, preferred_element_type=f32).astype(bf16)
    sent_cots = jnp.dot(placing, own_cots, preferred_element_type=f32).astype(bf16)
    sent_rows = sent_rows.reshape(groups, slot_span, quarter)
    sent_cots = sent_cots.reshape(groups, slot_span, quarter)
    padded = -(-slot_span // 128) * 128
    sent_weights = jnp.broadcast_to(
        jnp.pad(sent_weights, ((0, 0), (0, padded - slot_span)))[:, None, :], (groups, 8, padded)
    )
    got_rows, got_cots, got_weights = dispatch(sent_rows, sent_cots, sent_weights, groups, lanes)
    got_weights = got_weights[:, 0, :slot_span]
    grads_gate, grads_up, grads_down, terms = ([], [], [], [])
    entry_rows = got_rows.reshape(groups * capacity, model_width)
    entry_cots = got_cots.reshape(groups * capacity, model_width)
    entry_weights = got_weights.reshape(groups * capacity)
    grad_gate, grad_up, grad_down, partial_sum = expert_pass(
        entry_rows, entry_cots, entry_weights, gate_weight[0], up_weight[0], down_weight[0]
    )
    grads_gate.append(grad_gate)
    grads_up.append(grad_up)
    grads_down.append(grad_down)
    terms.append(partial_sum.astype(bf16).reshape(groups, capacity, model_width))
    expert_term = terms[0]
    returned = collect(expert_term, groups, lanes).reshape(slots, quarter)
    own_grad = jnp.einsum("st,sq->tq", placing, returned, preferred_element_type=f32)
    dnormed = gather_quarters(own_grad.astype(bf16), groups, lanes).astype(f32)
    scaled = dnormed * norm_gain
    resid_grad = (
        cotangent.astype(f32)
        + inv_rms * scaled
        - resid_wide * inv_rms**3 * jnp.mean(scaled * resid_wide, axis=1, keepdims=True)
    )
    grad_resid = resid_grad.astype(bf16)
    extended = jnp.concatenate([earlier, mixed], axis=0)
    conv = (
        taps[0] * extended[:token_count]
        + taps[1] * extended[1 : token_count + 1]
        + taps[2] * extended[2 : token_count + 2]
    )
    merged = (gate_b.astype(f32) * conv).astype(bf16)
    out_partial = jnp.einsum("td,tc->dc", grad_resid, merged, preferred_element_type=f32)
    grad_out_weight = reduce_rows(
        out_partial.astype(bf16).reshape(groups, model_width // groups, merged.shape[1]),
        groups,
        lanes,
    )
    dmerged = jnp.dot(grad_resid, out_weight, preferred_element_type=f32)
    grad_gate_b = (dmerged * conv).astype(bf16)
    dconv = dmerged * gate_b.astype(f32)
    later = passed_along(dconv[:2], "sp", -1)
    extended_grad = jnp.concatenate([dconv, later], axis=0)
    dmixed = (
        taps[2] * extended_grad[:token_count]
        + taps[1] * extended_grad[1 : token_count + 1]
        + taps[0] * extended_grad[2 : token_count + 2]
    )
    grad_gate_c = (dmixed * values_u.astype(f32)).astype(bf16)
    grad_values = (dmixed * gate_c.astype(f32)).astype(bf16)
    return (
        jnp.stack(grads_gate),
        jnp.stack(grads_up),
        jnp.stack(grads_down),
        grad_resid,
        grad_out_weight,
        grad_gate_b,
        grad_gate_c,
        grad_values,
    )


def solution(mesh):
    placed = (
        P("sp", None),
        P("sp", None),
        P(),
        P("sp", None),
        P("sp", None),
        P("sp", None, "tp"),
        P("sp", None, "tp"),
        P("sp", "tp", None),
        P(None, "tp"),
        P("sp", "tp"),
        P("sp", "tp"),
        P("sp", "tp"),
        P(None, "tp"),
    )
    return jax.shard_map(
        on_device,
        mesh=mesh,
        in_specs=placed,
        out_specs=(
            P("sp", None, "tp"),
            P("sp", None, "tp"),
            P("sp", "tp", None),
            P("sp", None),
            P("sp", "tp"),
            P("sp", "tp"),
            P("sp", "tp"),
            P("sp", "tp"),
        ),
        check_vma=False,
    )
```

profile of v0, /device:TPU:12, one launch (start us, length us, event | category | flops | bytes accessed | tf_op | source)
XLA Modules:
  0.0 269.2 jit_solution(17670718595064728071)
XLA Ops:
  0.6 1.2 convert_multiply_fusion.2
  1.8 3.4 %collective-permute-start = (f32[2,256]{1,0:T(2,128)S(1)}, f32[2,256]{1,0:T(2,128)S(1)}, u32[]{:S(2)}, u32[]{:S(2)}) collective-permute-start(f32[2,256]{1,0:T(2,128)S(1)} %slice.61), channel_id=1, source_target_pairs={{0,4},{4,8},{8,12},{12,16},{16,20},{20,24},{24,28},{1,5},{5,9},{9,... | collective-permute-start | bytes 6152 | tf_op jit(solution)/shard_map/ppermute | solution.py:16
  5.3 3.5 %convert_element_type.72 = f32[384,2048]{1,0:T(8,128)} convert(bf16[384,2048]{1,0:T(8,128)(2,1)} %param.13) | non-fusion elementwise | flops 786432 | bytes 4718592 | tf_op jit(solution)/shard_map/convert_element_type | solution.py:479
  9.7 3.1 %convolution_convert_fusion = bf16[1536,512]{1,0:T(8,128)(2,1)} fusion(s32[384]{0:T(512)S(1)} %get-tuple-element.17, s32[384]{0:T(512)S(1)} %get-tuple-element.16, bf16[384,2048]{1,0:T(8,128)(2,1)} %param.14, s32[]{:T(128)S(6)} %select_n.16), kind=kOutput, calls=%fused_computation.5 | convolution fusion | flops 606535680 | bytes 1969156 | tf_op jit(solution)/shard_map/dot_general | solution.py:507
  13.4 3.4 %convolution_convert_fusion.1 = bf16[1536,512]{1,0:T(8,128)(2,1)} fusion(s32[384]{0:T(512)S(1)} %get-tuple-element.17, s32[384]{0:T(512)S(1)} %get-tuple-element.16, f32[384,2048]{1,0:T(8,128)} %convert_element_type.72, s32[]{:T(128)S(6)} %select_n.16, f32[512]{0:T(512)S(1)} %dynamic-slice, f32[384]{0:T(512)S(1)} %get-tuple-element.29), kind=kOutput, calls=%fused_computation.6 | convolution fusion | flops 607125504 | bytes 2365956 | tf_op jit(solution)/shard_map/dot_general | solution.py:506
  17.4 90.7 %dispatch.1 = (bf16[8,192,2048]{2,1,0:T(8,128)(2,1)}, bf16[8,192,2048]{2,1,0:T(8,128)(2,1)}, f32[8,8,256]{2,1,0:T(8,128)}) custom-call(bf16[8,192,512]{2,1,0:T(8,128)(2,1)} %bitcast.49, bf16[8,192,512]{2,1,0:T(8,128)(2,1)} %bitcast.48, f32[8,8,256]{2,1,0:T(8,128)} %broadcast_in_dim.57.sent_weights), custom_call_target="tpu_custom_call" | custom-call | bytes 377487360 | tf_op jit(solution)/shard_map/dispatch/pallas_call | solution.py:185
  108.2 5.9 %fusion.17 = f32[1536,256]{1,0:T(8,128)} fusion(bf16[1536,2048]{1,0:T(8,128)(2,1)} %bitcast.57, bf16[1,2048,256]{2,1,0:T(8,128)(2,1)S(1)} %copy-done), kind=kOutput, calls=%fused_computation.32 | convolution fusion | flops 1610612736 | bytes 8912896 | tf_op jit(solution)/shard_map/dot_general | solution.py:435
  114.1 3.0 %fusion.20 = f32[1536,256]{1,0:T(8,128)} fusion(bf16[1536,2048]{1,0:T(8,128)(2,1)S(1)} %bitcast.58, bf16[1,2048,256]{2,1,0:T(8,128)(2,1)S(1)} %copy-done.6), kind=kOutput, calls=%fused_computation.35 | convolution fusion | flops 1610612736 | bytes 8912896 | tf_op jit(solution)/shard_map/dot_general | solution.py:436
  118.0 7.1 %convolution_bitcast_fusion = f32[1,256,2048]{2,1,0:T(8,128)} fusion(bf16[1536,2048]{1,0:T(8,128)(2,1)} %bitcast.63, f32[1536,256]{1,0:T(8,128)} %fusion.20, f32[1536]{0:T(1024)S(1)} %mul.171, f32[1536,256]{1,0:T(8,128)} %fusion.17), kind=kOutput, calls=%fused_computation.8 | convolution fusion | flops 1613365248 | bytes 11540480 | tf_op jit(solution)/shard_map/rf,rd->fd/dot_general | solution.py:440
  125.1 5.4 %multiply_convert_fusion.1 = (bf16[1536,256]{1,0:T(8,128)(2,1)S(1)}, bf16[1536,256]{1,0:T(8,128)(2,1)S(1)}) fusion(f32[1536,256]{1,0:T(8,128)S(1)} %copy-done.20, f32[1536,256]{1,0:T(8,128)S(1)} %copy-done.21, f32[1536]{0:T(1024)S(1)} %mul.171, bf16[1536,2048]{1,0:T(8,128)(2,1)} %bitcast.64, bf16[1,256,2048]{2,1,0:T(8,128)(2,1)S(1)} %copy-done.17), kind=kOutput, calls=%fused_computation.17 | convolution fusion | flops 1616117760 | bytes 12064768 | tf_op jit(solution)/shard_map/rd,fd->rf/dot_general | solution.py:442
  130.6 3.2 %convolution_bitcast_fusion.2 = f32[1,2048,256]{2,1,0:T(8,128)} fusion(bf16[1536,2048]{1,0:T(8,128)(2,1)S(1)} %bitcast.61, bf16[1536,256]{1,0:T(8,128)(2,1)S(1)} %get-tuple-element.23), kind=kOutput, calls=%fused_computation.10 | convolution fusion | flops 1610612736 | bytes 9175040 | tf_op jit(solution)/shard_map/rd,rf->df/dot_general | solution.py:447
  133.9 1.8 fusion.15
  135.7 3.5 %convolution_bitcast_fusion.1 = f32[1,2048,256]{2,1,0:T(8,128)} fusion(bf16[1536,2048]{1,0:T(8,128)(2,1)S(1)} %bitcast.62, bf16[1536,256]{1,0:T(8,128)(2,1)S(1)} %get-tuple-element.22), kind=kOutput, calls=%fused_computation.9 | convolution fusion | flops 1610612736 | bytes 9175040 | tf_op jit(solution)/shard_map/rd,rf->df/dot_general | solution.py:448
  139.2 3.1 %add_convert_fusion = bf16[1536,2048]{1,0:T(8,128)(2,1)S(1)} fusion(f32[1536,2048]{1,0:T(8,128)S(1)} %fusion.15, bf16[1536,256]{1,0:T(8,128)(2,1)} %copy-done.7, bf16[1,2048,256]{2,1,0:T(8,128)(2,1)S(1)} %copy-done.6), kind=kOutput, calls=%fused_computation | convolution fusion | flops 1616904192 | bytes 20709376 | tf_op jit(solution)/shard_map/rf,df->rd/dot_general | solution.py:449
  142.3 67.9 %collect.1 = bf16[8,192,512]{2,1,0:T(8,128)(2,1)S(1)} custom-call(bf16[8,192,2048]{2,1,0:T(8,128)(2,1)S(1)} %bitcast.46), custom_call_target="tpu_custom_call" | custom-call | bytes 157286400 | tf_op jit(solution)/shard_map/collect/pallas_call | solution.py:310
  210.2 1.6 fusion.6.mine
  211.8 14.8 %gather_quarters.1 = bf16[384,2048]{1,0:T(8,128)(2,1)} custom-call(bf16[384,512]{1,0:T(8,128)(2,1)} %fusion.6.mine), custom_call_target="tpu_custom_call" | custom-call | tf_op jit(solution)/shard_map/gather_quarters/pallas_call | solution.py:364
  226.6 2.2 multiply_reduce_fusion
  228.9 1.1 subtract_convert_fusion
  230.3 1.3 multiply_convert_fusion.4
  231.6 3.5 %collective-permute-start.1 = (f32[2,256]{1,0:T(2,128)S(1)}, f32[2,256]{1,0:T(2,128)S(1)}, u32[]{:S(2)}, u32[]{:S(2)}) collective-permute-start(f32[2,256]{1,0:T(2,128)S(1)} %slice.64), channel_id=1, source_target_pairs={{4,0},{8,4},{12,8},{16,12},{20,16},{24,20},{28,24},{5,1},{9,5},{13... | collective-permute-start | bytes 6152 | tf_op jit(solution)/shard_map/ppermute | solution.py:16
  235.1 1.7 convolution_convert_fusion.2
  236.8 29.1 %reduce_rows.1 = f32[256,256]{1,0:T(8,128)} custom-call(bf16[8,256,256]{2,1,0:T(8,128)(2,1)} %bitcast.50), custom_call_target="tpu_custom_call" | custom-call | tf_op jit(solution)/shard_map/reduce_rows/pallas_call | solution.py:417
  267.5 1.7 copy.24
  (72 shorter events, 5.0 us)
Async XLA Ops:
  0.6 107.5 %copy-start = (bf16[1,2048,256]{2,1,0:T(8,128)(2,1)S(1)}, bf16[1,2048,256]{2,1,0:T(8,128)(2,1)}, u32[]{:S(2)}) copy-start(bf16[1,2048,256]{2,1,0:T(8,128)(2,1)} %param.18) | copy-start | bytes 3145732
  1.8 3.5 %copy-start.10 = (f32[384,256]{1,0:T(8,128)}, f32[384,256]{1,0:T(8,128)S(1)}, u32[]{:S(2)}) copy-start(f32[384,256]{1,0:T(8,128)S(1)} %convert_multiply_fusion.2) | copy-start | bytes 1179652
  1.8 228.2 %collective-permute-start = (f32[2,256]{1,0:T(2,128)S(1)}, f32[2,256]{1,0:T(2,128)S(1)}, u32[]{:S(2)}, u32[]{:S(2)}) collective-permute-start(f32[2,256]{1,0:T(2,128)S(1)} %slice.61), channel_id=1, source_target_pairs={{0,4},{4,8},{8,12},{12,16},{16,20},{20,24},{24,28},{1,5},{5,9},{9,... | collective-permute-start | bytes 6152 | tf_op jit(solution)/shard_map/ppermute | solution.py:16
  5.3 3.6 %copy-start.1 = (bf16[384,2048]{1,0:T(8,128)(2,1)S(1)}, bf16[384,2048]{1,0:T(8,128)(2,1)}, u32[]{:S(2)}) copy-start(bf16[384,2048]{1,0:T(8,128)(2,1)} %param.13) | copy-start | bytes 4718596
  5.3 4.0 %copy-start.13 = (s32[384,2]{0,1:T(2,128)S(1)}, s32[384,2]{0,1:T(2,128)}, u32[]{:S(2)}) copy-start(s32[384,2]{0,1:T(2,128)} %param.16) | copy-start | bytes 9220
  5.3 4.2 %copy-start.14 = (f32[384,2]{0,1:T(2,128)S(1)}, f32[384,2]{0,1:T(2,128)}, u32[]{:S(2)}) copy-start(f32[384,2]{0,1:T(2,128)} %param.17) | copy-start | bytes 9220
  5.3 4.3 %copy-start.12 = (f32[2048]{0:T(1024)S(1)}, f32[2048]{0:T(1024)}, u32[]{:S(2)}) copy-start(f32[2048]{0:T(1024)} %param.15) | copy-start | bytes 24580
  108.1 5.9 %copy-start.6 = (bf16[1,2048,256]{2,1,0:T(8,128)(2,1)S(1)}, bf16[1,2048,256]{2,1,0:T(8,128)(2,1)}, u32[]{:S(2)}) copy-start(bf16[1,2048,256]{2,1,0:T(8,128)(2,1)} %param.19) | copy-start | bytes 3145732
  108.2 5.9 %copy-start.16 = (bf16[8,192,2048]{2,1,0:T(8,128)(2,1)S(1)}, bf16[8,192,2048]{2,1,0:T(8,128)(2,1)}, u32[]{:S(2)}) copy-start(bf16[8,192,2048]{2,1,0:T(8,128)(2,1)} %get-tuple-element.11) | copy-start | bytes 18874372
  118.0 7.1 %copy-start.17 = (bf16[1,256,2048]{2,1,0:T(8,128)(2,1)S(1)}, bf16[1,256,2048]{2,1,0:T(8,128)(2,1)}, u32[]{:S(2)}) copy-start(bf16[1,256,2048]{2,1,0:T(8,128)(2,1)} %param.20) | copy-start | bytes 3145732
  118.0 7.1 %copy-start.20 = (f32[1536,256]{1,0:T(8,128)S(1)}, f32[1536,256]{1,0:T(8,128)}, u32[]{:S(2)}) copy-start(f32[1536,256]{1,0:T(8,128)} %fusion.17) | copy-start | bytes 4718596
  118.0 7.1 %copy-start.21 = (f32[1536,256]{1,0:T(8,128)S(1)}, f32[1536,256]{1,0:T(8,128)}, u32[]{:S(2)}) copy-start(f32[1536,256]{1,0:T(8,128)} %fusion.20) | copy-start | bytes 4718596
  118.0 12.6 %slice-start = ((s8[6291456]{0:T(1024)(128)(4,1)}), s8[4194304]{0:T(1024)(128)(4,1)S(1)}, s32[]{:S(2)}) async-start(s8[6291456]{0:T(1024)(128)(4,1)} %bitcast.59), calls=%async_computation | async-start | bytes 8388608
  125.1 5.5 %slice-start.1 = ((s8[6291456]{0:T(1024)(128)(4,1)}), s8[2097152]{0:T(1024)(128)(4,1)S(1)}, s32[]{:S(2)}) async-start(s8[6291456]{0:T(1024)(128)(4,1)} %bitcast.59), calls=%async_computation.1 | async-start | bytes 4194304
  130.6 5.1 %copy-start.7 = (bf16[1536,256]{1,0:T(8,128)(2,1)}, bf16[1536,256]{1,0:T(8,128)(2,1)S(1)}, u32[]{:S(2)}) copy-start(bf16[1536,256]{1,0:T(8,128)(2,1)S(1)} %get-tuple-element.22) | copy-start | bytes 2359300
  211.8 14.8 %copy-start.2 = (bf16[384,2048]{1,0:T(8,128)(2,1)S(1)}, bf16[384,2048]{1,0:T(8,128)(2,1)}, u32[]{:S(2)}) copy-start(bf16[384,2048]{1,0:T(8,128)(2,1)} %param.13) | copy-start | bytes 4718596
  226.5 2.2 copy-start.3
  226.6 2.3 copy-start.4
  228.9 1.4 copy-start.18
  228.9 1.4 copy-start.19
  230.0 6.8 %copy-start.5 = (bf16[384,2048]{1,0:T(8,128)(2,1)}, bf16[384,2048]{1,0:T(8,128)(2,1)S(1)}, u32[]{:S(2)}) copy-start(bf16[384,2048]{1,0:T(8,128)(2,1)S(1)} %subtract_convert_fusion) | copy-start | bytes 4718596
  231.6 34.4 %copy-start.9 = (bf16[384,256]{1,0:T(8,128)(2,1)S(1)}, bf16[384,256]{1,0:T(8,128)(2,1)}, u32[]{:S(2)}) copy-start(bf16[384,256]{1,0:T(8,128)(2,1)} %param.23) | copy-start | bytes 589828
  231.6 34.4 %collective-permute-start.1 = (f32[2,256]{1,0:T(2,128)S(1)}, f32[2,256]{1,0:T(2,128)S(1)}, u32[]{:S(2)}, u32[]{:S(2)}) collective-permute-start(f32[2,256]{1,0:T(2,128)S(1)} %slice.64), channel_id=1, source_target_pairs={{4,0},{8,4},{12,8},{16,12},{20,16},{24,20},{28,24},{5,1},{9,5},{13... | collective-permute-start | bytes 6152 | tf_op jit(solution)/shard_map/ppermute | solution.py:16
  235.1 31.8 %copy-start.8 = (bf16[384,256]{1,0:T(8,128)(2,1)S(1)}, bf16[384,256]{1,0:T(8,128)(2,1)}, u32[]{:S(2)}) copy-start(bf16[384,256]{1,0:T(8,128)(2,1)} %param.24) | copy-start | bytes 589828
  (2 other events, 2.2 us)
where the time goes:
time: 270 us; the launch traced here: 269 us
  Pallas kernels  202 us (75%)
  matrix products  44.3 us (16%)
  other arithmetic  10.5 us (4%)
  starting transfers between devices  6.92 us (3%)
  local copies, waits for them, and re-layouts  3.98 us (1%)
    pallas_call x1, Pallas kernels, dispatch(): pl.pallas_call(functools.partial(dispatch_kernel, groups, lanes), out_sha...  90.7 us
    pallas_call x1, Pallas kernels, collect(): pl.pallas_call(functools.partial(collect_kernel, groups, lanes), out_shap...  67.9 us
    pallas_call x1, Pallas kernels, reduce_rows(): pl.pallas_call(functools.partial(reduce_kernel, groups, lanes), out_shape...  29.1 us
    pallas_call x1, Pallas kernels, gather_quarters(): pl.pallas_call(functools.partial(gather_kernel, groups, lanes), out_shape...  14.8 us
    dot_general x1, matrix products, expert_pass(): jnp.einsum('rf,rd->fd', hidden, entry_cots, preferred_element_type=f32)  7.11 us
    ppermute x2, starting transfers between devices, passed_along(): return lax.ppermute(array, axis, pairs)  6.92 us
    dot_general x1, matrix products, expert_pass(): gate_pre = jnp.dot(entry_rows, gate_mat, preferred_element_type=f32)  5.88 us
    dot_general x1, matrix products, expert_pass(): jnp.einsum('rd,fd->rf', entry_cots, down_mat, preferred_element_type=f32)  5.44 us
  transfers between devices with their start and end apart: 2, of which 0 were waited for; matrix products, arithmetic and copies ran while one was open for 20% of the time, Pallas kernels for 75%

commit v1 on v0

v1 whole, which is shorter than its diff:
```python
import functools

import jax
import jax.numpy as jnp
from jax import lax
from jax.experimental import pallas as pl
from jax.experimental.pallas import tpu as pltpu
from jax.sharding import PartitionSpec as P

norm_eps = 1e-06


def passed_along(array, axis, by):
    size = lax.axis_size(axis)
    pairs = [(i, i + by) for i in range(size) if 0 <= i + by < size]
    return lax.ppermute(array, axis, pairs)


def remote(source, target, send_sem, recv_sem, **device):
    return pltpu.make_async_remote_copy(
        src_ref=source,
        dst_ref=target,
        send_sem=send_sem,
        recv_sem=recv_sem,
        device_id=device,
        device_id_type=pl.DeviceIdType.MESH,
    )


def greet(groups, spot, core_peer, far_peer):
    barrier = pltpu.get_barrier_semaphore()

    def to_group(offset, carry):
        pl.semaphore_signal(
            barrier,
            inc=1,
            device_id={"sp": lax.rem(spot + offset, groups)},
            device_id_type=pl.DeviceIdType.MESH,
        )
        return carry

    lax.fori_loop(1, groups, to_group, 0)
    for peer in (core_peer, far_peer):
        pl.semaphore_signal(
            barrier, inc=1, device_id={"tp": peer}, device_id_type=pl.DeviceIdType.MESH
        )
    pl.semaphore_wait(barrier, groups + 1)


def expert_kernel(
    groups,
    width,
    lanes,
    normed,
    cots,
    info,
    gate_mat,
    up_mat,
    down_mat,
    returned,
    gate_out,
    up_out,
    down_out,
    infos,
    dense,
    to_mate,
    to_mate_own,
    rows,
    row_cots,
    hidden,
    dgate,
    dup,
    partial,
    from_core,
    to_far,
    from_far,
    summed,
    grad_a,
    grad_b,
    local_sem,
    send_i,
    recv_i,
    send_z,
    recv_z,
    send_y,
    recv_y,
    send_o,
    recv_o,
    send_x,
    recv_x,
    send_c,
    recv_c,
    send_f,
    recv_f,
    send_t,
    recv_t,
    send_r,
    recv_r,
    send_h,
    recv_h,
):
    f32 = jnp.float32
    bf16 = jnp.bfloat16
    spot, lane = lax.axis_index("sp"), lax.axis_index("tp")
    depth = groups // width
    z, y = lax.div(spot, width), lax.rem(spot, width)
    core = lax.rem(lane, 2)
    core_peer = lane + 1 - 2 * core
    far_peer = lax.rem(lane + lanes // 2, lanes)
    mate = spot + 1 - 2 * y
    token_count, model_width = normed.shape
    quarter = model_width // lanes
    half = model_width // 2
    span = rows.shape[1]
    given = (normed, cots)
    laid = (rows, row_cots)

    def columns(who, size):
        return pl.ds(pl.multiple_of(who * size, size), size)

    def part(ref, block, who):
        return ref.at[block, :, columns(who, quarter)]

    def source(side, level):
        return z + level * (2 * side - 1)

    def valid(side, level):
        at = source(side, level)
        there = jnp.logical_and(at >= 0, at < depth)
        return jnp.logical_and(there, jnp.logical_or(level > 0, side == 0))

    def onward(side):
        at = z + 1 - 2 * side
        return jnp.logical_and(at >= 0, at < depth)

    def block_of(side, level, line):
        return source(side, level) * width + lax.rem(y + line, width)

    def tell(offset):
        goal = lax.rem(spot + offset, groups)
        return remote(info, infos.at[spot], send_i.at[offset], recv_i.at[spot], sp=goal)

    def told(offset):
        origin = lax.rem(spot - offset + groups, groups)
        return remote(info, infos.at[origin], send_i.at[offset], recv_i.at[origin], sp=origin)

    def hop(k, at, side, own):
        held = dense.at[k, at]
        return remote(
            given[k].at[:, columns(lane, quarter)] if own else held,
            held,
            send_z.at[k, side, at],
            recv_z.at[k, at],
            sp=spot + width * (1 - 2 * side),
        )

    def over(k, at):
        return remote(
            to_mate.at[k, at],
            part(laid[k], at * width + y, lane),
            send_y.at[k, at],
            recv_y.at[k, at],
            sp=mate,
        )

    def over_own(k):
        return remote(
            to_mate_own.at[k],
            laid[k].at[spot, :, columns(core, half)],
            send_o.at[k],
            recv_o.at[k],
            sp=mate,
        )

    def far_copy(k, block):
        held = part(laid[k], block, lane)
        return remote(held, held, send_x.at[k, block], recv_x.at[k, block], tp=far_peer)

    def core_copy(k, block):
        held = part(laid[k], block, lane)
        return remote(held, held, send_c.at[k, block], recv_c.at[k, block], tp=core_peer)

    def half_copy(k):
        held = laid[k].at[mate, :, columns(core, half)]
        return remote(held, held, send_c.at[k, mate], recv_c.at[k, mate], tp=core_peer)

    def pass_copy(k, block):
        held = part(laid[k], block, far_peer)
        return remote(held, held, send_f.at[k, block], recv_f.at[k, block], tp=core_peer)

    def to_core(block, far):
        who = lax.rem(core_peer + far * (lanes // 2), lanes)
        return remote(
            part(partial, block, who),
            from_core.at[block, far],
            send_t.at[block, far],
            recv_t.at[block, far],
            tp=core_peer,
        )

    def to_far_peer(block):
        return remote(
            to_far.at[block],
            from_far.at[block],
            send_r.at[block],
            recv_r.at[block],
            tp=far_peer,
        )

    def home(block):
        return remote(
            summed.at[block], returned.at[spot], send_h.at[block], recv_h.at[spot], sp=block
        )

    def home_from(block):
        return remote(
            summed.at[block], returned.at[block], send_h.at[block], recv_h.at[block], sp=block
        )

    def matches(block, expert):
        slot = lax.broadcasted_iota(jnp.int32, (span, token_count), 0) + expert * span
        slot = slot.astype(f32)
        return slot == infos[block, 0:1, :], slot == infos[block, 1:2, :]

    def chosen(block, expert):
        first, second = matches(block, expert)
        return jnp.where(jnp.logical_or(first, second), 1.0, 0.0).astype(bf16)

    def weights_of(block):
        first, second = matches(block, spot)
        return jnp.sum(
            jnp.where(first, infos[block, 2:3, :], 0.0)
            + jnp.where(second, infos[block, 3:4, :], 0.0),
            axis=1,
            keepdims=True,
        )

    def placed(matrix, values):
        return jnp.dot(matrix, values, preferred_element_type=f32).astype(bf16)

    def both(body):
        def step(side, carry):
            body(side)
            return carry

        lax.fori_loop(0, 2, step, 0)

    def each_block(level, body):
        def step(at, carry):
            side, line = lax.div(at, 2), lax.rem(at, 2)

            @pl.when(valid(side, level))
            def _():
                body(block_of(side, level, line), side, line)

            return carry

        lax.fori_loop(0, 4, step, 0)

    core_side, far_side = core_peer, far_peer
    greet(groups, spot, core_side, far_side)

    def tell_all(offset, carry):
        tell(offset).start()
        return carry

    lax.fori_loop(1, groups, tell_all, 0)
    for k in (0, 1):
        for side in (0, 1):

            @pl.when(onward(side))
            def _():
                hop(k, z, side, True).start()

    infos[spot] = info[...]
    mine_there = chosen(spot, mate)
    for k in (0, 1):
        to_mate_own[k] = placed(mine_there, given[k][:, columns(core, half)])
        over_own(k).start()
    mine_here = chosen(spot, spot)

    def lay_own(at, carry):
        for k in (0, 1):
            laid[k][spot, :, columns(at, quarter)] = placed(
                mine_here, given[k][:, columns(at, quarter)]
            )
        return carry

    lax.fori_loop(0, lanes, lay_own, 0)

    def hear_all(offset, carry):
        told(offset).wait_recv()
        return carry

    lax.fori_loop(1, groups, hear_all, 0)

    def dispatch_level(level):
        for k in (0, 1):

            def take(side):
                @pl.when(valid(side, level))
                def _():
                    at = source(side, level)
                    hop(k, at, side, False).wait_recv()

                    @pl.when(onward(side))
                    def _():
                        hop(k, at, side, False).start()

            both(take)

            def place(side):
                @pl.when(valid(side, level))
                def _():
                    at = source(side, level)
                    block = at * width + y
                    values = dense[k, at]
                    to_mate[k, at] = placed(chosen(block, mate), values)
                    over(k, at).start()
                    laid[k][block, :, columns(lane, quarter)] = placed(
                        chosen(block, spot), values
                    )
                    far_copy(k, block).start()
                    core_copy(k, block).start()

            both(place)

        def receive(side):
            @pl.when(valid(side, level))
            def _():
                at = source(side, level)
                block = at * width + 1 - y
                for k in (0, 1):
                    over(k, at).wait_recv()
                    far_copy(k, block).start()
                    core_copy(k, block).start()

        both(receive)

    def share_level(level):
        @pl.when(level == 0)
        def _():
            for k in (0, 1):
                over_own(k).wait_recv()
                half_copy(k).start()

        def share(block, side, line):
            @pl.when(level > 0)
            def _():
                for k in (0, 1):
                    far_copy(k, block).wait_recv()
                    pass_copy(k, block).start()

        each_block(level, share)

    def compute_level(level):
        def compute(block, side, line):
            @pl.when(level > 0)
            def _():
                for k in (0, 1):
                    core_copy(k, block).wait_recv()
                    pass_copy(k, block).wait_recv()

            @pl.when(jnp.logical_and(level == 0, line == 1))
            def _():
                for k in (0, 1):
                    half_copy(k).wait_recv()

            weight = weights_of(block)
            entry_rows = rows[block]
            gate_pre = jnp.dot(entry_rows, gate_mat[...], preferred_element_type=f32)
            up_pre = jnp.dot(entry_rows, up_mat[...], preferred_element_type=f32)
            pulled = lax.dot_general(
                row_cots[block],
                down_mat[...],
                (((1,), (1,)), ((), ())),
                preferred_element_type=f32,
            )
            logistic = jax.nn.sigmoid(gate_pre)
            activated = gate_pre * logistic
            hidden[block] = (activated * up_pre * weight).astype(bf16)
            dhidden = pulled * weight
            grad_gate = (
                dhidden * up_pre * logistic * (1.0 + gate_pre * (1.0 - logistic))
            ).astype(bf16)
            grad_up = (dhidden * activated).astype(bf16)
            dgate[block] = grad_gate
            dup[block] = grad_up

            def back(at, carry):
                picked = columns(at, quarter)
                over_width = (((1,), (1,)), ((), ()))
                partial[block, :, picked] = (
                    lax.dot_general(
                        grad_gate, gate_mat[picked, :], over_width, preferred_element_type=f32
                    )
                    + lax.dot_general(
                        grad_up, up_mat[picked, :], over_width, preferred_element_type=f32
                    )
                ).astype(bf16)
                return carry

            lax.fori_loop(0, lanes, back, 0)
            to_core(block, 1).start()
            to_core(block, 0).start()

        each_block(level, compute)

    def middle_level(level):
        def middle(block, side, line):
            to_core(block, 1).wait_recv()
            to_far[block] = (
                partial[block, :, columns(far_peer, quarter)].astype(f32)
                + from_core[block, 1].astype(f32)
            ).astype(bf16)
            to_far_peer(block).start()

        each_block(level, middle)

    def total_level(level):
        def total(block, side, line):
            to_core(block, 0).wait_recv()
            to_far_peer(block).wait_recv()
            value = (
                partial[block, :, columns(lane, quarter)].astype(f32)
                + from_core[block, 0].astype(f32)
                + from_far[block].astype(f32)
            ).astype(bf16)

            @pl.when(block == spot)
            def _():
                returned[spot] = value

            @pl.when(block != spot)
            def _():
                summed[block] = value
                home(block).start()

        each_block(level, total)

    def weight_grads():
        slots = groups * span
        down_in = (((0,), (0,)), ((), ()))

        def down_step(at, carry):
            picked = columns(at, quarter)
            grad_b[:, picked] = lax.dot_general(
                hidden[...].reshape(slots, hidden.shape[2]),
                row_cots[:, :, picked].reshape(slots, quarter),
                down_in,
                preferred_element_type=f32,
            )
            return carry

        lax.fori_loop(0, lanes, down_step, 0)
        down_copy = pltpu.make_async_copy(grad_b, down_out, local_sem.at[0])
        down_copy.start()
        copies = [down_copy]
        for spread, out, index in ((dgate, gate_out, 0), (dup, up_out, 1)):

            def step(at, carry):
                picked = columns(at, quarter)
                grad_a[index, picked, :] = lax.dot_general(
                    rows[:, :, picked].reshape(slots, quarter),
                    spread[...].reshape(slots, spread.shape[2]),
                    down_in,
                    preferred_element_type=f32,
                )
                return carry

            lax.fori_loop(0, lanes, step, 0)
            copy = pltpu.make_async_copy(grad_a.at[index], out, local_sem.at[index + 1])
            copy.start()
            copies.append(copy)
        for copy in copies:
            copy.wait()

    def advance(level, carry):
        dispatch_level(level)
        share_level(level - 1)
        compute_level(level - 1)

        @pl.when(level >= 2)
        def _():
            middle_level(level - 2)

        @pl.when(level >= 3)
        def _():
            total_level(level - 3)

        return carry

    lax.fori_loop(1, depth + 1, advance, 0)
    middle_level(depth - 1)
    total_level(depth - 2)
    weight_grads()
    total_level(depth - 1)

    def finish_info(offset, carry):
        tell(offset).wait_send()
        origin = lax.rem(spot + offset, groups)
        home_from(origin).wait()
        return carry

    lax.fori_loop(1, groups, finish_info, 0)
    for k in (0, 1):
        for side in (0, 1):

            @pl.when(onward(side))
            def _():
                hop(k, z, side, True).wait_send()

        over_own(k).wait_send()
        half_copy(k).wait_send()

    def finish_level(level, carry):
        def finish(block, side, line):
            to_core(block, 0).wait_send()
            to_core(block, 1).wait_send()
            to_far_peer(block).wait_send()

            @pl.when(level > 0)
            def _():
                for k in (0, 1):
                    far_copy(k, block).wait_send()
                    core_copy(k, block).wait_send()
                    pass_copy(k, block).wait_send()

            @pl.when(jnp.logical_and(level > 0, line == 0))
            def _():
                at = source(side, level)
                for k in (0, 1):
                    over(k, at).wait_send()

                    @pl.when(onward(side))
                    def _():
                        hop(k, at, side, False).wait_send()

        each_block(level, finish)
        return carry

    lax.fori_loop(0, depth, finish_level, 0)


def experts(normed, cots, info, gate_mat, up_mat, down_mat, groups, lanes, span):
    token_count, model_width = normed.shape
    inner = gate_mat.shape[1]
    quarter = model_width // lanes
    width = 2
    depth = groups // width
    bf16, f32 = jnp.bfloat16, jnp.float32
    dma = pltpu.SemaphoreType.DMA
    inside = pl.BlockSpec(memory_space=pltpu.VMEM)
    anywhere = pl.BlockSpec(memory_space=pl.ANY)
    block = (groups, span, quarter)
    whole = (groups, span, model_width)
    thin = (groups, span, inner)
    vmem = pltpu.VMEM
    return pl.pallas_call(
        functools.partial(expert_kernel, groups, width, lanes),
        out_shape=(
            jax.ShapeDtypeStruct(block, bf16),
            jax.ShapeDtypeStruct(gate_mat.shape, f32),
            jax.ShapeDtypeStruct(up_mat.shape, f32),
            jax.ShapeDtypeStruct(down_mat.shape, f32),
        ),
        in_specs=[inside] * 6,
        out_specs=(inside, anywhere, anywhere, anywhere),
        scratch_shapes=[
            vmem((groups,) + info.shape, f32),
            vmem((2, depth, token_count, quarter), bf16),
            vmem((2, depth, span, quarter), bf16),
            vmem((2, span, model_width // 2), bf16),
            vmem(whole, bf16),
            vmem(whole, bf16),
            vmem(thin, bf16),
            vmem(thin, bf16),
            vmem(thin, bf16),
            vmem(whole, bf16),
            vmem((groups, 2, span, quarter), bf16),
            vmem(block, bf16),
            vmem(block, bf16),
            vmem(block, bf16),
            vmem((2,) + gate_mat.shape, f32),
            vmem(down_mat.shape, f32),
            dma((3,)),
            dma((groups,)),
            dma((groups,)),
            dma((2, 2, depth)),
            dma((2, depth)),
            dma((2, depth)),
            dma((2, depth)),
            dma((2,)),
            dma((2,)),
        ]
        + [dma((2, groups))] * 6
        + [dma((groups, 2))] * 2
        + [dma((groups,))] * 4,
        compiler_params=pltpu.CompilerParams(
            collective_id=1, has_side_effects=True, vmem_limit_bytes=63 * 2**20
        ),
        cost_estimate=pl.CostEstimate(
            flops=16 * groups * span * model_width * inner,
            bytes_accessed=150 * 2**20,
            transcendentals=0,
        ),
        name="experts",
    )(normed, cots, info, gate_mat, up_mat, down_mat)


def gather_kernel(groups, lanes, mine, gathered, own_sem, send_sems, recv_sems):
    spot, lane = lax.axis_index("sp"), lax.axis_index("tp")
    core_peer = lane + 1 - 2 * lax.rem(lane, 2)
    far_peer = lax.rem(lane + lanes // 2, lanes)
    quarter = mine.shape[1]

    def part(who):
        return gathered.at[:, pl.ds(pl.multiple_of(who * quarter, quarter), quarter)]

    greet(groups, spot, core_peer, far_peer)
    far = remote(mine, part(lane), send_sems.at[0], recv_sems.at[0], tp=far_peer)
    near = remote(mine, part(lane), send_sems.at[1], recv_sems.at[1], tp=core_peer)
    own = pltpu.make_async_copy(mine, part(lane), own_sem)
    far.start()
    near.start()
    own.start()
    far.wait_recv()
    passed = remote(
        part(far_peer), part(far_peer), send_sems.at[2], recv_sems.at[2], tp=core_peer
    )
    passed.start()
    far.wait_send()
    near.wait()
    own.wait()
    passed.wait()


def gather_quarters(mine, groups, lanes):
    sem = pltpu.SemaphoreType.DMA
    inside = pl.BlockSpec(memory_space=pltpu.VMEM)
    return pl.pallas_call(
        functools.partial(gather_kernel, groups, lanes),
        out_shape=jax.ShapeDtypeStruct((mine.shape[0], mine.shape[1] * lanes), mine.dtype),
        in_specs=[inside],
        out_specs=inside,
        scratch_shapes=[sem, sem((3,)), sem((3,))],
        compiler_params=pltpu.CompilerParams(collective_id=3, has_side_effects=True),
        name="gather_quarters",
    )(mine)


def reduce_kernel(groups, lanes, partial, total, arrived, send_sems, recv_sems):
    f32 = jnp.float32
    spot, lane = lax.axis_index("sp"), lax.axis_index("tp")
    core_peer = lane + 1 - 2 * lax.rem(lane, 2)
    far_peer = lax.rem(lane + lanes // 2, lanes)

    def across(offset):
        goal = lax.rem(spot + offset, groups)
        return remote(
            partial.at[goal],
            arrived.at[offset],
            send_sems.at[offset],
            recv_sems.at[offset],
            sp=goal,
        )

    greet(groups, spot, core_peer, far_peer)

    def launch(offset, carry):
        across(offset).start()
        return carry

    lax.fori_loop(1, groups, launch, 0)
    total[...] = partial[spot].astype(f32)

    def add(offset, carry):
        across(offset).wait_recv()
        total[...] += arrived[offset].astype(f32)
        return carry

    lax.fori_loop(1, groups, add, 0)

    def finish(offset, carry):
        across(offset).wait_send()
        return carry

    lax.fori_loop(1, groups, finish, 0)


def reduce_rows(partial, groups, lanes):
    sem = pltpu.SemaphoreType.DMA
    inside = pl.BlockSpec(memory_space=pltpu.VMEM)
    return pl.pallas_call(
        functools.partial(reduce_kernel, groups, lanes),
        out_shape=jax.ShapeDtypeStruct(partial.shape[1:], jnp.float32),
        in_specs=[inside],
        out_specs=inside,
        scratch_shapes=[
            pltpu.VMEM(partial.shape, partial.dtype),
            sem((groups,)),
            sem((groups,)),
        ],
        compiler_params=pltpu.CompilerParams(collective_id=4, has_side_effects=True),
        name="reduce_rows",
    )(partial)


def on_device(
    resid_in,
    cotangent,
    norm_gain,
    routes,
    route_weights,
    gate_weight,
    up_weight,
    down_weight,
    out_weight,
    gate_b,
    gate_c,
    values_u,
    taps,
):
    f32 = jnp.float32
    bf16 = jnp.bfloat16
    token_count, model_width = resid_in.shape
    groups = lax.axis_size("sp")
    lanes = lax.axis_size("tp")
    local_experts = gate_weight.shape[0]
    expert_total = local_experts * groups
    capacity = 4 * token_count // expert_total
    slot_span = local_experts * capacity
    resid_wide = resid_in.astype(f32)
    inv_rms = lax.rsqrt(jnp.mean(resid_wide * resid_wide, axis=1, keepdims=True) + norm_eps)
    normed = (resid_wide * inv_rms * norm_gain).astype(bf16)
    mixed = gate_c.astype(f32) * values_u.astype(f32)
    earlier = passed_along(mixed[-2:], "sp", 1)
    quarter = model_width // lanes
    slots = expert_total * capacity
    names = jnp.arange(expert_total, dtype=jnp.int32)
    chosen = routes[:, :, None] == names[None, None, :]
    named = jnp.any(chosen, axis=1).astype(bf16)
    order = jnp.arange(token_count, dtype=jnp.int32)
    strict = (order[:, None] > order[None, :]).astype(bf16)
    before = jnp.dot(strict, named, preferred_element_type=f32).astype(jnp.int32)
    rank = jnp.sum(jnp.where(chosen, before[:, None, :], 0), axis=2)
    targets = routes * capacity + rank
    slot_ids = jnp.arange(slots, dtype=jnp.int32)[:, None]
    first = slot_ids == targets[:, 0][None, :]
    second = slot_ids == targets[:, 1][None, :]
    placing = (first | second).astype(bf16)
    info = jnp.concatenate(
        [
            targets.T.astype(f32),
            route_weights.T,
            jnp.zeros((4, token_count), f32),
        ],
        axis=0,
    )
    returned, grad_gate, grad_up, grad_down = experts(
        normed,
        cotangent,
        info,
        gate_weight[0],
        up_weight[0],
        down_weight[0],
        groups,
        lanes,
        slot_span,
    )
    returned = returned.reshape(slots, quarter)
    own_grad = jnp.einsum("st,sq->tq", placing, returned, preferred_element_type=f32)
    dnormed = gather_quarters(own_grad.astype(bf16), groups, lanes).astype(f32)
    scaled = dnormed * norm_gain
    resid_grad = (
        cotangent.astype(f32)
        + inv_rms * scaled
        - resid_wide * inv_rms**3 * jnp.mean(scaled * resid_wide, axis=1, keepdims=True)
    )
    grad_resid = resid_grad.astype(bf16)
    extended = jnp.concatenate([earlier, mixed], axis=0)
    conv = (
        taps[0] * extended[:token_count]
        + taps[1] * extended[1 : token_count + 1]
        + taps[2] * extended[2 : token_count + 2]
    )
    merged = (gate_b.astype(f32) * conv).astype(bf16)
    out_partial = jnp.einsum("td,tc->dc", grad_resid, merged, preferred_element_type=f32)
    grad_out_weight = reduce_rows(
        out_partial.astype(bf16).reshape(groups, model_width // groups, merged.shape[1]),
        groups,
        lanes,
    )
    dmerged = jnp.dot(grad_resid, out_weight, preferred_element_type=f32)
    grad_gate_b = (dmerged * conv).astype(bf16)
    dconv = dmerged * gate_b.astype(f32)
    later = passed_along(dconv[:2], "sp", -1)
    extended_grad = jnp.concatenate([dconv, later], axis=0)
    dmixed = (
        taps[2] * extended_grad[:token_count]
        + taps[1] * extended_grad[1 : token_count + 1]
        + taps[0] * extended_grad[2 : token_count + 2]
    )
    grad_gate_c = (dmixed * values_u.astype(f32)).astype(bf16)
    grad_values = (dmixed * gate_c.astype(f32)).astype(bf16)
    return (
        grad_gate[None],
        grad_up[None],
        grad_down[None],
        grad_resid,
        grad_out_weight,
        grad_gate_b,
        grad_gate_c,
        grad_values,
    )


def solution(mesh):
    placed = (
        P("sp", None),
        P("sp", None),
        P(),
        P("sp", None),
        P("sp", None),
        P("sp", None, "tp"),
        P("sp", None, "tp"),
        P("sp", "tp", None),
        P(None, "tp"),
        P("sp", "tp"),
        P("sp", "tp"),
        P("sp", "tp"),
        P(None, "tp"),
    )
    return jax.shard_map(
        on_device,
        mesh=mesh,
        in_specs=placed,
        out_specs=(
            P("sp", None, "tp"),
            P("sp", None, "tp"),
            P("sp", "tp", None),
            P("sp", None),
            P("sp", "tp"),
            P("sp", "tp"),
            P("sp", "tp"),
            P("sp", "tp"),
        ),
        check_vma=False,
    )
```

time: 270 us -> 208 us (0.77)
  matrix products: 44.3 us -> 6.9 us
  Pallas kernels: 202 us -> 176 us
  local copies, waits for them, and re-layouts: 3.98 us -> 7.61 us
    dot_general x10 -> x0, matrix products: 39.6 us -> none  [the longest x1 7.11 us: expert_pass(): jnp.einsum('rf,rd->fd', hidden, entry_cots, preferred_element_type=f32)]
    pallas_call x2 -> x1, Pallas kernels: 159 us -> 130 us  [experts(): pl.pallas_call(functools.partial(expert_kernel, groups, width, lanes), ou...]
    unnamed x49 -> x38, local copies, waits for them, and re-layouts: 2.19 us -> 6.92 us
  transfers between devices with their start and end apart: 2 -> 2, of which waited for: 0 -> 0; matrix products, arithmetic and copies ran while one was open for 20% -> 6% of each run, Pallas kernels for 75% -> 85%
where the time goes in v1:
time: 208 us
  Pallas kernels  176 us (85%)
  other arithmetic  10 us (5%)
  local copies, waits for them, and re-layouts  7.61 us (4%)
  matrix products  6.9 us (3%)
  starting transfers between devices  6.11 us (3%)
    pallas_call x1, Pallas kernels, experts(): pl.pallas_call(functools.partial(expert_kernel, groups, width, lanes), ou...  130 us
    pallas_call x1, Pallas kernels, reduce_rows(): pl.pallas_call(functools.partial(reduce_kernel, groups, lanes), out_shape...  29.3 us
    pallas_call x1, Pallas kernels, gather_quarters(): pl.pallas_call(functools.partial(gather_kernel, groups, lanes), out_shape...  17.3 us
    unnamed x38, local copies, waits for them, and re-layouts  6.92 us
    ppermute x2, starting transfers between devices, passed_along(): return lax.ppermute(array, axis, pairs)  6.11 us
  transfers between devices with their start and end apart: 2, of which 0 were waited for; matrix products, arithmetic and copies ran while one was open for 6% of the time, Pallas kernels for 85%

profile of v1, /device:TPU:12, one launch (start us, length us, event | category | flops | bytes accessed | tf_op | source)
XLA Modules:
  0.0 207.7 jit_solution(16441461560073603531)
XLA Ops:
  0.7 1.2 convert_multiply_fusion.6
  1.8 0.6 slice.49
  2.4 3.5 %collective-permute-start = (f32[2,256]{1,0:T(2,128)}, f32[2,256]{1,0:T(2,128)}, u32[]{:S(2)}, u32[]{:S(2)}) collective-permute-start(f32[2,256]{1,0:T(2,128)} %slice.49), channel_id=1, source_target_pairs={{0,4},{4,8},{8,12},{12,16},{16,20},{20,24},{24,28},{1,5},{5,9},{9,... | collective-permute-start | bytes 6152 | tf_op jit(solution)/shard_map/ppermute | solution.py:16
  6.0 1.8 fusion
  7.8 0.1 convolution_convert_fusion.1
  8.1 1.6 fusion.2.normed
  9.7 0.7 maximum_maximum_fusion.info
  10.4 129.6 %experts.1 = (bf16[8,192,512]{2,1,0:T(8,128)(2,1)}, f32[2048,256]{1,0:T(8,128)}, f32[2048,256]{1,0:T(8,128)}, f32[256,2048]{1,0:T(8,128)}) custom-call(bf16[384,2048]{1,0:T(8,128)(2,1)} %fusion.2.normed, bf16[384,2048]{1,0:T(8,128)(2,1)} %cots.1, f32[8,384]{1,0:T(8,128)} %maximum_maximum_fusion.info, bf16[2048,256]{1,0:T(8,128)(2,1)} %bitcast.30, ...), custom_call_target="tpu_custom_call" | custom-call | flops 12884901888 | bytes 157286400 | tf_op jit(solution)/shard_map/experts/pallas_call | solution.py:559
  140.0 3.0 %fusion.10.mine = bf16[384,512]{1,0:T(8,128)(2,1)} fusion(bf16[1536,512]{1,0:T(8,128)(2,1)} %bitcast.33, s32[384]{0:T(512)S(1)} %get-tuple-element.17, s32[384]{0:T(512)S(1)} %get-tuple-element.16), kind=kOutput, calls=%fused_computation.17 | convolution fusion | flops 605945856 | bytes 1969152 | tf_op jit(solution)/shard_map/st,sq->tq/dot_general | solution.py:772
  143.0 17.3 %gather_quarters.1 = bf16[384,2048]{1,0:T(8,128)(2,1)} custom-call(bf16[384,512]{1,0:T(8,128)(2,1)} %fusion.10.mine), custom_call_target="tpu_custom_call" | custom-call | tf_op jit(solution)/shard_map/gather_quarters/pallas_call | solution.py:641
  160.3 2.1 %fusion.6 = f32[384]{0:T(512)S(1)} fusion(bf16[384,2048]{1,0:T(8,128)(2,1)S(1)} %copy-done.1, bf16[384,2048]{1,0:T(8,128)(2,1)} %gather_quarters.1, f32[2048]{0:T(1024)S(1)} %copy-done.11), kind=kLoop, calls=%fused_computation.10 | loop fusion | flops 3931776 | bytes 3155456 | tf_op jit(solution)/shard_map/reduce_sum | solution.py:778
  162.5 1.0 fusion.5
  163.7 2.0 multiply_convert_fusion
  165.8 2.6 %collective-permute-start.1 = (f32[2,256]{1,0:T(2,128)S(1)}, f32[2,256]{1,0:T(2,128)S(1)}, u32[]{:S(2)}, u32[]{:S(2)}) collective-permute-start(f32[2,256]{1,0:T(2,128)S(1)} %slice.52), channel_id=1, source_target_pairs={{4,0},{8,4},{12,8},{16,12},{20,16},{24,20},{28,24},{5,1},{9,5},{13... | collective-permute-start | bytes 6152 | tf_op jit(solution)/shard_map/ppermute | solution.py:16
  168.4 1.7 convolution_convert_fusion
  170.1 29.3 %reduce_rows.1 = f32[256,256]{1,0:T(8,128)} custom-call(bf16[8,256,256]{2,1,0:T(8,128)(2,1)} %bitcast.22), custom_call_target="tpu_custom_call" | custom-call | tf_op jit(solution)/shard_map/reduce_rows/pallas_call | solution.py:694
  199.4 0.8 fusion.24
  200.2 0.7 fusion.25
  200.9 1.3 copy.27
  202.3 1.0 copy-done.4
  203.3 1.3 copy.28
  204.6 1.0 copy-done.3
  205.6 1.3 copy.29
  207.0 0.7 copy.30
  (44 shorter events, 0.4 us)
Async XLA Ops:
  0.6 7.4 %copy-start = (bf16[384,2048]{1,0:T(8,128)(2,1)S(1)}, bf16[384,2048]{1,0:T(8,128)(2,1)}, u32[]{:S(2)}) copy-start(bf16[384,2048]{1,0:T(8,128)(2,1)} %param.13) | copy-start | bytes 4718596
  0.6 7.1 %copy-start.12 = (s32[384,2]{0,1:T(2,128)S(1)}, s32[384,2]{0,1:T(2,128)}, u32[]{:S(2)}) copy-start(s32[384,2]{0,1:T(2,128)} %param.16) | copy-start | bytes 9220
  0.7 7.4 %copy-start.11 = (f32[2048]{0:T(1024)S(1)}, f32[2048]{0:T(1024)}, u32[]{:S(2)}) copy-start(f32[2048]{0:T(1024)} %param.15) | copy-start | bytes 24580
  2.4 7.3 %copy-start.13 = (f32[384,2]{0,1:T(2,128)S(1)}, f32[384,2]{0,1:T(2,128)}, u32[]{:S(2)}) copy-start(f32[384,2]{0,1:T(2,128)} %param.17) | copy-start | bytes 9220
  2.4 161.1 %collective-permute-start = (f32[2,256]{1,0:T(2,128)}, f32[2,256]{1,0:T(2,128)}, u32[]{:S(2)}, u32[]{:S(2)}) collective-permute-start(f32[2,256]{1,0:T(2,128)} %slice.49), channel_id=1, source_target_pairs={{0,4},{4,8},{8,12},{12,16},{16,20},{20,24},{24,28},{1,5},{5,9},{9,... | collective-permute-start | bytes 6152 | tf_op jit(solution)/shard_map/ppermute | solution.py:16
  143.0 17.3 %copy-start.1 = (bf16[384,2048]{1,0:T(8,128)(2,1)S(1)}, bf16[384,2048]{1,0:T(8,128)(2,1)}, u32[]{:S(2)}) copy-start(bf16[384,2048]{1,0:T(8,128)(2,1)} %param.13) | copy-start | bytes 4718596
  143.0 19.4 %copy-start.6 = (bf16[384,2048]{1,0:T(8,128)(2,1)S(1)}, bf16[384,2048]{1,0:T(8,128)(2,1)}, u32[]{:S(2)}) copy-start(bf16[384,2048]{1,0:T(8,128)(2,1)} %cots.1) | copy-start | bytes 4718596
  160.3 2.1 %copy-start.2 = (bf16[384,2048]{1,0:T(8,128)(2,1)S(1)}, bf16[384,2048]{1,0:T(8,128)(2,1)}, u32[]{:S(2)}) copy-start(bf16[384,2048]{1,0:T(8,128)(2,1)} %gather_quarters.1) | copy-start | bytes 4718596
  162.4 1.1 copy-start.14
  162.5 1.2 copy-start.15
  162.5 1.2 copy-start.16
  163.5 4.8 %copy-start.7 = (bf16[384,2048]{1,0:T(8,128)(2,1)}, bf16[384,2048]{1,0:T(8,128)(2,1)S(1)}, u32[]{:S(2)}) copy-start(bf16[384,2048]{1,0:T(8,128)(2,1)S(1)} %fusion.5) | copy-start | bytes 4718596
  165.8 33.6 %collective-permute-start.1 = (f32[2,256]{1,0:T(2,128)S(1)}, f32[2,256]{1,0:T(2,128)S(1)}, u32[]{:S(2)}, u32[]{:S(2)}) collective-permute-start(f32[2,256]{1,0:T(2,128)S(1)} %slice.52), channel_id=1, source_target_pairs={{4,0},{8,4},{12,8},{16,12},{20,16},{24,20},{28,24},{5,1},{9,5},{13... | collective-permute-start | bytes 6152 | tf_op jit(solution)/shard_map/ppermute | solution.py:16
  168.3 31.0 %copy-start.10 = (bf16[384,256]{1,0:T(8,128)(2,1)S(1)}, bf16[384,256]{1,0:T(8,128)(2,1)}, u32[]{:S(2)}) copy-start(bf16[384,256]{1,0:T(8,128)(2,1)} %param.23) | copy-start | bytes 589828
  168.3 31.9 %copy-start.9 = (bf16[384,256]{1,0:T(8,128)(2,1)S(1)}, bf16[384,256]{1,0:T(8,128)(2,1)}, u32[]{:S(2)}) copy-start(bf16[384,256]{1,0:T(8,128)(2,1)} %param.24) | copy-start | bytes 589828
  170.1 30.9 %copy-start.5 = (f32[2048,256]{1,0:T(8,128)S(1)}, f32[2048,256]{1,0:T(8,128)}, u32[]{:S(2)}) copy-start(f32[2048,256]{1,0:T(8,128)} %get-tuple-element.12) | copy-start | bytes 6291460
  200.9 2.3 %copy-start.4 = (f32[2048,256]{1,0:T(8,128)S(1)}, f32[2048,256]{1,0:T(8,128)}, u32[]{:S(2)}) copy-start(f32[2048,256]{1,0:T(8,128)} %get-tuple-element.13) | copy-start | bytes 6291460
  203.3 2.3 %copy-start.3 = (f32[256,2048]{1,0:T(8,128)S(1)}, f32[256,2048]{1,0:T(8,128)}, u32[]{:S(2)}) copy-start(f32[256,2048]{1,0:T(8,128)} %get-tuple-element.14) | copy-start | bytes 6291460
  205.6 1.3 copy-start.8

commit v2 on v1

--- a/solution.py
+++ b/solution.py
@@ -54,16 +54,19 @@
     normed,
     cots,
     info,
+    targets,
     gate_mat,
     up_mat,
     down_mat,
-    returned,
+    gathered,
     gate_out,
     up_out,
     down_out,
     infos,
     dense,
+    dense_wide,
     to_mate,
+    to_mate_wide,
     to_mate_own,
     rows,
     row_cots,
@@ -75,6 +78,8 @@
     to_far,
     from_far,
     summed,
+    returned,
+    combined,
     grad_a,
     grad_b,
     local_sem,
@@ -98,6 +103,8 @@
     recv_r,
     send_h,
     recv_h,
+    send_g,
+    recv_g,
 ):
     f32 = jnp.float32
     bf16 = jnp.bfloat16
@@ -126,15 +133,19 @@
 
     def valid(side, level):
         at = source(side, level)
-        there = jnp.logical_and(at >= 0, at < depth)
-        return jnp.logical_and(there, jnp.logical_or(level > 0, side == 0))
+        return jnp.logical_and(level > 0, jnp.logical_and(at >= 0, at < depth))
+
+    def present(side, level, line):
+        near = jnp.logical_and(side == 0, line == level + 1)
+        return jnp.logical_or(valid(side, level), jnp.logical_and(level <= 0, near))
 
     def onward(side):
         at = z + 1 - 2 * side
         return jnp.logical_and(at >= 0, at < depth)
 
     def block_of(side, level, line):
-        return source(side, level) * width + lax.rem(y + line, width)
+        at = source(side, lax.max(level, 0))
+        return at * width + lax.rem(y + line, width)
 
     def tell(offset):
         goal = lax.rem(spot + offset, groups)
@@ -143,6 +154,40 @@
     def told(offset):
         origin = lax.rem(spot - offset + groups, groups)
         return remote(info, infos.at[origin], send_i.at[offset], recv_i.at[origin], sp=origin)
+
+    def is_end(at):
+        return jnp.logical_or(at == 0, at == depth - 1)
+
+    def end_of(at):
+        return lax.min(at, 1)
+
+    def by_kind(at, wide, narrow):
+        @pl.when(is_end(at))
+        def _():
+            wide()
+
+        @pl.when(jnp.logical_not(is_end(at)))
+        def _():
+            narrow()
+
+    def hop_wide(k, at, side, own):
+        held = dense_wide.at[k, end_of(at)]
+        return remote(
+            given[k].at[:, columns(core, half)] if own else held,
+            held,
+            send_z.at[k, side, at],
+            recv_z.at[k, at],
+            sp=spot + width * (1 - 2 * side),
+        )
+
+    def over_wide(k, at):
+        return remote(
+            to_mate_wide.at[k, end_of(at)],
+            laid[k].at[at * width + y, :, columns(core, half)],
+            send_y.at[k, at],
+            recv_y.at[k, at],
+            sp=mate,
+        )
 
     def hop(k, at, side, own):
         held = dense.at[k, at]
@@ -180,9 +225,9 @@
         held = part(laid[k], block, lane)
         return remote(held, held, send_c.at[k, block], recv_c.at[k, block], tp=core_peer)
 
-    def half_copy(k):
-        held = laid[k].at[mate, :, columns(core, half)]
-        return remote(held, held, send_c.at[k, mate], recv_c.at[k, mate], tp=core_peer)
+    def half_copy(k, block):
+        held = laid[k].at[block, :, columns(core, half)]
+        return remote(held, held, send_c.at[k, block], recv_c.at[k, block], tp=core_peer)
 
     def pass_copy(k, block):
         held = part(laid[k], block, far_peer)
@@ -249,7 +294,7 @@
         def step(at, carry):
             side, line = lax.div(at, 2), lax.rem(at, 2)
 
-            @pl.when(valid(side, level))
+            @pl.when(present(side, level, line))
             def _():
                 body(block_of(side, level, line), side, line)
 
@@ -270,7 +315,11 @@
 
             @pl.when(onward(side))
             def _():
-                hop(k, z, side, True).start()
+                by_kind(
+                    z,
+                    lambda: hop_wide(k, z, side, True).start(),
+                    lambda: hop(k, z, side, True).start(),
+                )
 
     infos[spot] = info[...]
     mine_there = chosen(spot, mate)
@@ -288,52 +337,79 @@
 
     lax.fori_loop(0, lanes, lay_own, 0)
 
-    def hear_all(offset, carry):
-        told(offset).wait_recv()
-        return carry
-
-    lax.fori_loop(1, groups, hear_all, 0)
-
-    def dispatch_level(level):
-        for k in (0, 1):
-
-            def take(side):
-                @pl.when(valid(side, level))
-                def _():
-                    at = source(side, level)
-                    hop(k, at, side, False).wait_recv()
-
-                    @pl.when(onward(side))
-                    def _():
-                        hop(k, at, side, False).start()
-
-            both(take)
-
-            def place(side):
-                @pl.when(valid(side, level))
-                def _():
-                    at = source(side, level)
-                    block = at * width + y
-                    values = dense[k, at]
-                    to_mate[k, at] = placed(chosen(block, mate), values)
-                    over(k, at).start()
-                    laid[k][block, :, columns(lane, quarter)] = placed(
-                        chosen(block, spot), values
-                    )
-                    far_copy(k, block).start()
-                    core_copy(k, block).start()
-
-            both(place)
-
+    def move(copy, k, at, side):
+        copy(k, at, side, False).wait_recv()
+
+        @pl.when(onward(side))
+        def _():
+            copy(k, at, side, False).start()
+
+    def at_ends(level, ends, body):
+        def step(side):
+            at = source(side, level)
+            kind = is_end(at) if ends else jnp.logical_not(is_end(at))
+
+            @pl.when(jnp.logical_and(valid(side, level), kind))
+            def _():
+                body(side, at, at * width + y)
+
+        both(step)
+
+    def early(side, level):
+        return jnp.logical_and(onward(side), level >= 2)
+
+    def take_narrow(level, k):
+        def body(side, at, block):
+            move(hop, k, at, side)
+            values = dense[k, at]
+            laid[k][block, :, columns(lane, quarter)] = placed(chosen(block, spot), values)
+            far_copy(k, block).start()
+            core_copy(k, block).start()
+            to_mate[k, at] = placed(chosen(block, mate), values)
+            over(k, at).start()
+
+        at_ends(level, False, body)
+
+    def move_early(level, k):
+        def body(side, at, block):
+            @pl.when(early(side, level))
+            def _():
+                move(hop_wide, k, at, side)
+
+        at_ends(level, True, body)
+
+    def take_wide(level, k):
+        def body(side, at, block):
+            @pl.when(jnp.logical_not(early(side, level)))
+            def _():
+                move(hop_wide, k, at, side)
+
+            end = end_of(at)
+            values = dense_wide[k, end]
+            to_mate_wide[k, end] = placed(chosen(block, mate), values)
+            over_wide(k, at).start()
+            laid[k][block, :, columns(core, half)] = placed(chosen(block, spot), values)
+            half_copy(k, block).start()
+
+        at_ends(level, True, body)
+
+    def receive_level(level, k):
         def receive(side):
             @pl.when(valid(side, level))
             def _():
                 at = source(side, level)
                 block = at * width + 1 - y
-                for k in (0, 1):
+
+                def wide():
+                    over_wide(k, at).wait_recv()
+                    half_copy(k, block).start()
+
+                def narrow():
                     over(k, at).wait_recv()
                     far_copy(k, block).start()
                     core_copy(k, block).start()
+
+                by_kind(at, wide, narrow)
 
         both(receive)
 
@@ -342,10 +418,12 @@
         def _():
             for k in (0, 1):
                 over_own(k).wait_recv()
-                half_copy(k).start()
+                half_copy(k, mate).start()
 
         def share(block, side, line):
-            @pl.when(level > 0)
+            narrow = jnp.logical_not(is_end(source(side, level)))
+
+            @pl.when(jnp.logical_and(level > 0, narrow))
             def _():
                 for k in (0, 1):
                     far_copy(k, block).wait_recv()
@@ -357,14 +435,21 @@
         def compute(block, side, line):
             @pl.when(level > 0)
             def _():
+                def wide():
+                    for k in (0, 1):
+                        half_copy(k, block).wait_recv()
+
+                def narrow():
+                    for k in (0, 1):
+                        core_copy(k, block).wait_recv()
+                        pass_copy(k, block).wait_recv()
+
+                by_kind(source(side, level), wide, narrow)
+
+            @pl.when(jnp.logical_and(level == 0, line == 1))
+            def _():
                 for k in (0, 1):
-                    core_copy(k, block).wait_recv()
-                    pass_copy(k, block).wait_recv()
-
-            @pl.when(jnp.logical_and(level == 0, line == 1))
-            def _():
-                for k in (0, 1):
-                    half_copy(k).wait_recv()
+                    half_copy(k, mate).wait_recv()
 
             weight = weights_of(block)
             entry_rows = rows[block]
@@ -476,30 +561,74 @@
             copy.wait()
 
     def advance(level, carry):
-        dispatch_level(level)
+        @pl.when(level == 1)
+        def _():
+            def hear_all(offset, carry):
+                told(offset).wait_recv()
+                return carry
+
+            lax.fori_loop(1, groups, hear_all, 0)
+
+        take_narrow(level, 0)
+        take_narrow(level, 1)
+        take_wide(level, 0)
         share_level(level - 1)
+        move_early(level, 1)
         compute_level(level - 1)
-
-        @pl.when(level >= 2)
+        middle_level(level - 1)
+        take_wide(level, 1)
+        move_early(level + 1, 0)
+        receive_level(level, 0)
+
+        @pl.when(level < depth)
         def _():
-            middle_level(level - 2)
-
-        @pl.when(level >= 3)
-        def _():
-            total_level(level - 3)
-
+            total_level(level - 1)
+
+        receive_level(level, 1)
         return carry
 
-    lax.fori_loop(1, depth + 1, advance, 0)
-    middle_level(depth - 1)
-    total_level(depth - 2)
+    lax.fori_loop(0, depth + 1, advance, 0)
     weight_grads()
     total_level(depth - 1)
+    combined[...] = jnp.zeros_like(combined)
+
+    def combine_level(level, carry):
+        def combine(block, side, line):
+            @pl.when(block != spot)
+            def _():
+                home_from(block).wait_recv()
+
+            slot = lax.broadcasted_iota(jnp.int32, (token_count, span), 1) + block * span
+            slot = slot.astype(f32)
+            hit = jnp.logical_or(slot == targets[:, 0:1], slot == targets[:, 1:2])
+            picked = jnp.where(hit, 1.0, 0.0).astype(bf16)
+            combined[...] += jnp.dot(picked, returned[block], preferred_element_type=f32)
+
+        each_block(level, combine)
+        return carry
+
+    lax.fori_loop(-1, depth, combine_level, 0)
+
+    def gather_part(who):
+        return gathered.at[:, columns(who, quarter)]
+
+    def gather_copy(index, who, peer):
+        held = gather_part(who)
+        return remote(held, held, send_g.at[index], recv_g.at[index], tp=peer)
+
+    gathered[:, columns(lane, quarter)] = combined[...].astype(bf16)
+    gather_copy(0, lane, far_peer).start()
+    gather_copy(1, lane, core_peer).start()
+    gather_copy(0, lane, far_peer).wait_recv()
+    gather_copy(2, far_peer, core_peer).start()
+    gather_copy(0, lane, far_peer).wait_send()
+    gather_copy(1, lane, core_peer).wait()
+    gather_copy(2, far_peer, core_peer).wait()
 
     def finish_info(offset, carry):
         tell(offset).wait_send()
         origin = lax.rem(spot + offset, groups)
-        home_from(origin).wait()
+        home_from(origin).wait_send()
         return carry
 
     lax.fori_loop(1, groups, finish_info, 0)
@@ -508,10 +637,14 @@
 
             @pl.when(onward(side))
             def _():
-                hop(k, z, side, True).wait_send()
+                by_kind(
+                    z,
+                    lambda: hop_wide(k, z, side, True).wait_send(),
+                    lambda: hop(k, z, side, True).wait_send(),
+                )
 
         over_own(k).wait_send()
-        half_copy(k).wait_send()
+        half_copy(k, mate).wait_send()
 
     def finish_level(level, carry):
         def finish(block, side, line):
@@ -521,28 +654,39 @@
 
             @pl.when(level > 0)
             def _():
-                for k in (0, 1):
-                    far_copy(k, block).wait_send()
-                    core_copy(k, block).wait_send()
-                    pass_copy(k, block).wait_send()
-
-            @pl.when(jnp.logical_and(level > 0, line == 0))
-            def _():
                 at = source(side, level)
-                for k in (0, 1):
-                    over(k, at).wait_send()
-
-                    @pl.when(onward(side))
+
+                def done(hold, cross):
+                    @pl.when(line == 0)
                     def _():
-                        hop(k, at, side, False).wait_send()
+                        for k in (0, 1):
+                            cross(k, at).wait_send()
+
+                            @pl.when(onward(side))
+                            def _():
+                                hold(k, at, side, False).wait_send()
+
+                def wide():
+                    for k in (0, 1):
+                        half_copy(k, block).wait_send()
+                    done(hop_wide, over_wide)
+
+                def narrow():
+                    for k in (0, 1):
+                        far_copy(k, block).wait_send()
+                        core_copy(k, block).wait_send()
+                        pass_copy(k, block).wait_send()
+                    done(hop, over)
+
+                by_kind(at, wide, narrow)
 
         each_block(level, finish)
         return carry
 
-    lax.fori_loop(0, depth, finish_level, 0)
-
-
-def experts(normed, cots, info, gate_mat, up_mat, down_mat, groups, lanes, span):
+    lax.fori_loop(-1, depth, finish_level, 0)
+
+
+def experts(normed, cots, info, targets, gate_mat, up_mat, down_mat, groups, lanes, span):
     token_count, model_width = normed.shape
     inner = gate_mat.shape[1]
     quarter = model_width // lanes
@@ -559,17 +703,19 @@
     return pl.pallas_call(
         functools.partial(expert_kernel, groups, width, lanes),
         out_shape=(
-            jax.ShapeDtypeStruct(block, bf16),
+            jax.ShapeDtypeStruct(normed.shape, bf16),
             jax.ShapeDtypeStruct(gate_mat.shape, f32),
             jax.ShapeDtypeStruct(up_mat.shape, f32),
             jax.ShapeDtypeStruct(down_mat.shape, f32),
         ),
-        in_specs=[inside] * 6,
+        in_specs=[inside] * 7,
         out_specs=(inside, anywhere, anywhere, anywhere),
         scratch_shapes=[
             vmem((groups,) + info.shape, f32),
             vmem((2, depth, token_count, quarter), bf16),
+            vmem((2, 2, token_count, model_width // 2), bf16),
             vmem((2, depth, span, quarter), bf16),
+            vmem((2, 2, span, model_width // 2), bf16),
             vmem((2, span, model_width // 2), bf16),
             vmem(whole, bf16),
             vmem(whole, bf16),
@@ -581,6 +727,8 @@
             vmem(block, bf16),
             vmem(block, bf16),
             vmem(block, bf16),
+            vmem(block, bf16),
+            vmem((token_count, quarter), f32),
             vmem((2,) + gate_mat.shape, f32),
             vmem(down_mat.shape, f32),
             dma((3,)),
@@ -595,7 +743,8 @@
         ]
         + [dma((2, groups))] * 6
         + [dma((groups, 2))] * 2
-        + [dma((groups,))] * 4,
+        + [dma((groups,))] * 4
+        + [dma((3,))] * 2,
         compiler_params=pltpu.CompilerParams(
             collective_id=1, has_side_effects=True, vmem_limit_bytes=63 * 2**20
         ),
@@ -605,48 +754,7 @@
             transcendentals=0,
         ),
         name="experts",
-    )(normed, cots, info, gate_mat, up_mat, down_mat)
-
-
-def gather_kernel(groups, lanes, mine, gathered, own_sem, send_sems, recv_sems):
-    spot, lane = lax.axis_index("sp"), lax.axis_index("tp")
-    core_peer = lane + 1 - 2 * lax.rem(lane, 2)
-    far_peer = lax.rem(lane + lanes // 2, lanes)
-    quarter = mine.shape[1]
-
-    def part(who):
-        return gathered.at[:, pl.ds(pl.multiple_of(who * quarter, quarter), quarter)]
-
-    greet(groups, spot, core_peer, far_peer)
-    far = remote(mine, part(lane), send_sems.at[0], recv_sems.at[0], tp=far_peer)
-    near = remote(mine, part(lane), send_sems.at[1], recv_sems.at[1], tp=core_peer)
-    own = pltpu.make_async_copy(mine, part(lane), own_sem)
-    far.start()
-    near.start()
-    own.start()
-    far.wait_recv()
-    passed = remote(
-        part(far_peer), part(far_peer), send_sems.at[2], recv_sems.at[2], tp=core_peer
-    )
-    passed.start()
-    far.wait_send()
-    near.wait()
-    own.wait()
-    passed.wait()
-
-
-def gather_quarters(mine, groups, lanes):
-    sem = pltpu.SemaphoreType.DMA
-    inside = pl.BlockSpec(memory_space=pltpu.VMEM)
-    return pl.pallas_call(
-        functools.partial(gather_kernel, groups, lanes),
-        out_shape=jax.ShapeDtypeStruct((mine.shape[0], mine.shape[1] * lanes), mine.dtype),
-        in_specs=[inside],
-        out_specs=inside,
-        scratch_shapes=[sem, sem((3,)), sem((3,))],
-        compiler_params=pltpu.CompilerParams(collective_id=3, has_side_effects=True),
-        name="gather_quarters",
-    )(mine)
+    )(normed, cots, info, targets, gate_mat, up_mat, down_mat)
 
 
 def reduce_kernel(groups, lanes, partial, total, arrived, send_sems, recv_sems):
@@ -735,8 +843,6 @@
     normed = (resid_wide * inv_rms * norm_gain).astype(bf16)
     mixed = gate_c.astype(f32) * values_u.astype(f32)
     earlier = passed_along(mixed[-2:], "sp", 1)
-    quarter = model_width // lanes
-    slots = expert_total * capacity
     names = jnp.arange(expert_total, dtype=jnp.int32)
     chosen = routes[:, :, None] == names[None, None, :]
     named = jnp.any(chosen, axis=1).astype(bf16)
@@ -745,10 +851,6 @@
     before = jnp.dot(strict, named, preferred_element_type=f32).astype(jnp.int32)
     rank = jnp.sum(jnp.where(chosen, before[:, None, :], 0), axis=2)
     targets = routes * capacity + rank
-    slot_ids = jnp.arange(slots, dtype=jnp.int32)[:, None]
-    first = slot_ids == targets[:, 0][None, :]
-    second = slot_ids == targets[:, 1][None, :]
-    placing = (first | second).astype(bf16)
     info = jnp.concatenate(
         [
             targets.T.astype(f32),
@@ -757,10 +859,11 @@
         ],
         axis=0,
     )
-    returned, grad_gate, grad_up, grad_down = experts(
+    gathered, grad_gate, grad_up, grad_down = experts(
         normed,
         cotangent,
         info,
+        targets.astype(f32),
         gate_weight[0],
         up_weight[0],
         down_weight[0],
@@ -768,9 +871,7 @@
         lanes,
         slot_span,
     )
-    returned = returned.reshape(slots, quarter)
-    own_grad = jnp.einsum("st,sq->tq", placing, returned, preferred_element_type=f32)
-    dnormed = gather_quarters(own_grad.astype(bf16), groups, lanes).astype(f32)
+    dnormed = gathered.astype(f32)
     scaled = dnormed * norm_gain
     resid_grad = (
         cotangent.astype(f32)

time: 208 us -> 193 us (0.928)
  Pallas kernels: 176 us -> 162 us
  matrix products: 6.9 us -> 3.17 us
  other arithmetic: 10 us -> 12.7 us
    pallas_call x1 -> x0, Pallas kernels: 17.3 us -> none  [gather_quarters(): pl.pallas_call(functools.partial(gather_kernel, groups, lanes), out_shape...]
    pallas_call x1, Pallas kernels: 29.3 us -> 33.3 us  [reduce_rows(): pl.pallas_call(functools.partial(reduce_kernel, groups, lanes), out_shape...]
    dot_general x1 -> x0, matrix products: 2.98 us -> none  [on_device(): jnp.einsum('st,sq->tq', placing, returned, preferred_element_type=f32)]
    unnamed x38 -> x36, local copies, waits for them, and re-layouts: 6.92 us -> 6.95 us
  transfers between devices with their start and end apart: 2 -> 2, of which waited for: 0 -> 0; matrix products, arithmetic and copies ran while one was open for 6% -> 6% of each run, Pallas kernels for 85% -> 84%
where the time goes in v2:
time: 193 us
  Pallas kernels  162 us (84%)
  other arithmetic  12.7 us (7%)
  local copies, waits for them, and re-layouts  7.26 us (4%)
  starting transfers between devices  6.4 us (3%)
  matrix products  3.17 us (2%)
    pallas_call x1, Pallas kernels, experts(): pl.pallas_call(functools.partial(expert_kernel, groups, width, lanes), ou...  129 us
    pallas_call x1, Pallas kernels, reduce_rows(): pl.pallas_call(functools.partial(reduce_kernel, groups, lanes), out_shape...  33.3 us
    unnamed x36, local copies, waits for them, and re-layouts  6.95 us
    ppermute x2, starting transfers between devices, passed_along(): return lax.ppermute(array, axis, pairs)  6.4 us
  transfers between devices with their start and end apart: 2, of which 0 were waited for; matrix products, arithmetic and copies ran while one was open for 6% of the time, Pallas kernels for 84%

profile of v2, /device:TPU:12, one launch (start us, length us, event | category | flops | bytes accessed | tf_op | source)
XLA Modules:
  0.0 192.5 jit_solution(10025252810744087270)
XLA Ops:
  0.7 1.2 convert_multiply_fusion.6
  1.9 3.4 %collective-permute-start = (f32[2,256]{1,0:T(2,128)S(1)}, f32[2,256]{1,0:T(2,128)S(1)}, u32[]{:S(2)}, u32[]{:S(2)}) collective-permute-start(f32[2,256]{1,0:T(2,128)S(1)} %slice.39), channel_id=1, source_target_pairs={{0,4},{4,8},{8,12},{12,16},{16,20},{20,24},{24,28},{1,5},{5,9},{9,... | collective-permute-start | bytes 6152 | tf_op jit(solution)/shard_map/ppermute | solution.py:16
  5.3 1.8 fusion
  7.1 0.1 convolution_convert_fusion.1
  7.3 0.1 copy.31
  7.5 0.7 fusion.24
  8.3 1.6 fusion.2.normed
  10.0 0.7 maximum_maximum_fusion.info
  10.6 128.8 %experts.1 = (bf16[384,2048]{1,0:T(8,128)(2,1)}, f32[2048,256]{1,0:T(8,128)}, f32[2048,256]{1,0:T(8,128)}, f32[256,2048]{1,0:T(8,128)}) custom-call(bf16[384,2048]{1,0:T(8,128)(2,1)} %fusion.2.normed, bf16[384,2048]{1,0:T(8,128)(2,1)} %cots.1, f32[8,384]{1,0:T(8,128)} %maximum_maximum_fusion.info, f32[384,2]{1,0:T(8,128)} %get-tuple-element.21.targets, ...), custom_call_target="tpu_custom_call" | custom-call | flops 12884901888 | bytes 157286400 | tf_op jit(solution)/shard_map/experts/pallas_call | solution.py:703
  139.5 2.6 %fusion.6 = f32[384]{0:T(512)S(1)} fusion(bf16[384,2048]{1,0:T(8,128)(2,1)} %param.13, bf16[384,2048]{1,0:T(8,128)(2,1)} %get-tuple-element.15, f32[2048]{0:T(1024)S(1)} %copy-done.10), kind=kLoop, calls=%fused_computation.10 | loop fusion | flops 3931776 | bytes 3155456 | tf_op jit(solution)/shard_map/reduce_sum | solution.py:879
  142.1 0.2 copy-done.2
  142.3 2.5 %fusion.5 = bf16[384,2048]{1,0:T(8,128)(2,1)S(1)} fusion(bf16[384,2048]{1,0:T(8,128)(2,1)S(1)} %copy-done.1, bf16[384,2048]{1,0:T(8,128)(2,1)S(1)} %copy-done.2, bf16[384,2048]{1,0:T(8,128)(2,1)} %cots.1, f32[384]{0:T(512)S(1)} %broadcast_multiply_fusion, f32[384]{0:T(512)S(1)} %get-tuple-element.26, f32[2048]{0:T(1024)S(1)} %copy-done.10, ...), kind=kLoop, calls=%fused_computation.9 | loop fusion | flops 7864320 | bytes 6304256 | tf_op jit(solution)/shard_map/convert_element_type | solution.py:881
  144.9 1.3 multiply_convert_fusion
  146.2 3.0 %collective-permute-start.1 = (f32[2,256]{1,0:T(2,128)S(1)}, f32[2,256]{1,0:T(2,128)S(1)}, u32[]{:S(2)}, u32[]{:S(2)}) collective-permute-start(f32[2,256]{1,0:T(2,128)S(1)} %slice.42), channel_id=1, source_target_pairs={{4,0},{8,4},{12,8},{16,12},{20,16},{24,20},{28,24},{5,1},{9,5},{13... | collective-permute-start | bytes 6152 | tf_op jit(solution)/shard_map/ppermute | solution.py:16
  149.2 1.7 convolution_convert_fusion
  150.9 33.3 %reduce_rows.1 = f32[256,256]{1,0:T(8,128)} custom-call(bf16[8,256,256]{2,1,0:T(8,128)(2,1)} %bitcast.20), custom_call_target="tpu_custom_call" | custom-call | tf_op jit(solution)/shard_map/reduce_rows/pallas_call | solution.py:802
  184.2 0.8 fusion.16
  185.1 0.7 fusion.17
  185.8 1.3 copy.37
  187.1 1.0 copy-done.4
  188.2 1.3 copy.38
  189.5 1.0 copy-done.3
  190.5 1.3 copy.39
  191.8 0.7 copy.40
  (42 shorter events, 0.3 us)
Async XLA Ops:
  0.6 7.7 %copy-start = (bf16[384,2048]{1,0:T(8,128)(2,1)S(1)}, bf16[384,2048]{1,0:T(8,128)(2,1)}, u32[]{:S(2)}) copy-start(bf16[384,2048]{1,0:T(8,128)(2,1)} %param.13) | copy-start | bytes 4718596
  0.6 6.5 %copy-start.11 = (s32[384,2]{0,1:T(2,128)S(1)}, s32[384,2]{0,1:T(2,128)}, u32[]{:S(2)}) copy-start(s32[384,2]{0,1:T(2,128)} %param.16) | copy-start | bytes 9220
  0.7 7.6 %copy-start.10 = (f32[2048]{0:T(1024)S(1)}, f32[2048]{0:T(1024)}, u32[]{:S(2)}) copy-start(f32[2048]{0:T(1024)} %param.15) | copy-start | bytes 24580
  1.9 143.0 %collective-permute-start = (f32[2,256]{1,0:T(2,128)S(1)}, f32[2,256]{1,0:T(2,128)S(1)}, u32[]{:S(2)}, u32[]{:S(2)}) collective-permute-start(f32[2,256]{1,0:T(2,128)S(1)} %slice.39), channel_id=1, source_target_pairs={{0,4},{4,8},{8,12},{12,16},{16,20},{20,24},{24,28},{1,5},{5,9},{9,... | collective-permute-start | bytes 6152 | tf_op jit(solution)/shard_map/ppermute | solution.py:16
  7.3 2.7 %copy-start.12 = (f32[384,2]{0,1:T(2,128)S(1)}, f32[384,2]{0,1:T(2,128)}, u32[]{:S(2)}) copy-start(f32[384,2]{0,1:T(2,128)} %param.17) | copy-start | bytes 9220
  139.4 2.7 %copy-start.1 = (bf16[384,2048]{1,0:T(8,128)(2,1)S(1)}, bf16[384,2048]{1,0:T(8,128)(2,1)}, u32[]{:S(2)}) copy-start(bf16[384,2048]{1,0:T(8,128)(2,1)} %param.13) | copy-start | bytes 4718596
  139.5 2.8 %copy-start.2 = (bf16[384,2048]{1,0:T(8,128)(2,1)S(1)}, bf16[384,2048]{1,0:T(8,128)(2,1)}, u32[]{:S(2)}) copy-start(bf16[384,2048]{1,0:T(8,128)(2,1)} %get-tuple-element.15) | copy-start | bytes 4718596
  142.3 2.5 %copy-start.13 = (f32[3,256]{1,0:T(4,128)S(1)}, f32[3,256]{1,0:T(4,128)}, u32[]{:S(2)}) copy-start(f32[3,256]{1,0:T(4,128)} %param.25) | copy-start | bytes 9220
  142.3 2.6 %copy-start.14 = (bf16[2048,256]{1,0:T(8,128)(2,1)S(1)}, bf16[2048,256]{1,0:T(8,128)(2,1)}, u32[]{:S(2)}) copy-start(bf16[2048,256]{1,0:T(8,128)(2,1)} %param.21) | copy-start | bytes 3145732
  142.3 2.6 %copy-start.15 = (bf16[384,256]{1,0:T(8,128)(2,1)S(1)}, bf16[384,256]{1,0:T(8,128)(2,1)}, u32[]{:S(2)}) copy-start(bf16[384,256]{1,0:T(8,128)(2,1)} %param.22) | copy-start | bytes 589828
  144.8 4.3 %copy-start.6 = (bf16[384,2048]{1,0:T(8,128)(2,1)}, bf16[384,2048]{1,0:T(8,128)(2,1)S(1)}, u32[]{:S(2)}) copy-start(bf16[384,2048]{1,0:T(8,128)(2,1)S(1)} %fusion.5) | copy-start | bytes 4718596
  146.2 38.0 %collective-permute-start.1 = (f32[2,256]{1,0:T(2,128)S(1)}, f32[2,256]{1,0:T(2,128)S(1)}, u32[]{:S(2)}, u32[]{:S(2)}) collective-permute-start(f32[2,256]{1,0:T(2,128)S(1)} %slice.42), channel_id=1, source_target_pairs={{4,0},{8,4},{12,8},{16,12},{20,16},{24,20},{28,24},{5,1},{9,5},{13... | collective-permute-start | bytes 6152 | tf_op jit(solution)/shard_map/ppermute | solution.py:16
  149.2 35.1 %copy-start.9 = (bf16[384,256]{1,0:T(8,128)(2,1)S(1)}, bf16[384,256]{1,0:T(8,128)(2,1)}, u32[]{:S(2)}) copy-start(bf16[384,256]{1,0:T(8,128)(2,1)} %param.23) | copy-start | bytes 589828
  149.2 35.9 %copy-start.8 = (bf16[384,256]{1,0:T(8,128)(2,1)S(1)}, bf16[384,256]{1,0:T(8,128)(2,1)}, u32[]{:S(2)}) copy-start(bf16[384,256]{1,0:T(8,128)(2,1)} %param.24) | copy-start | bytes 589828
  150.9 34.9 %copy-start.5 = (f32[2048,256]{1,0:T(8,128)S(1)}, f32[2048,256]{1,0:T(8,128)}, u32[]{:S(2)}) copy-start(f32[2048,256]{1,0:T(8,128)} %get-tuple-element.12) | copy-start | bytes 6291460
  185.8 2.3 %copy-start.4 = (f32[2048,256]{1,0:T(8,128)S(1)}, f32[2048,256]{1,0:T(8,128)}, u32[]{:S(2)}) copy-start(f32[2048,256]{1,0:T(8,128)} %get-tuple-element.13) | copy-start | bytes 6291460
  188.2 2.3 %copy-start.3 = (f32[256,2048]{1,0:T(8,128)S(1)}, f32[256,2048]{1,0:T(8,128)}, u32[]{:S(2)}) copy-start(f32[256,2048]{1,0:T(8,128)} %get-tuple-element.14) | copy-start | bytes 6291460
  190.5 1.3 copy-start.7

commit v3 on v2

--- a/solution.py
+++ b/solution.py
@@ -8,12 +8,6 @@
 from jax.sharding import PartitionSpec as P
 
 norm_eps = 1e-06
-
-
-def passed_along(array, axis, by):
-    size = lax.axis_size(axis)
-    pairs = [(i, i + by) for i in range(size) if 0 <= i + by < size]
-    return lax.ppermute(array, axis, pairs)
 
 
 def remote(source, target, send_sem, recv_sem, **device):
@@ -51,17 +45,24 @@
     groups,
     width,
     lanes,
-    normed,
+    resid,
     cots,
+    gain,
+    edge,
     info,
     targets,
     gate_mat,
     up_mat,
     down_mat,
-    gathered,
+    resid_grad,
+    edge_got,
     gate_out,
     up_out,
     down_out,
+    normed,
+    inverse,
+    product,
+    gathered,
     infos,
     dense,
     dense_wide,
@@ -77,7 +78,6 @@
     from_core,
     to_far,
     from_far,
-    summed,
     returned,
     combined,
     grad_a,
@@ -105,6 +105,8 @@
     recv_h,
     send_g,
     recv_g,
+    send_e,
+    recv_e,
 ):
     f32 = jnp.float32
     bf16 = jnp.bfloat16
@@ -115,10 +117,12 @@
     core_peer = lane + 1 - 2 * core
     far_peer = lax.rem(lane + lanes // 2, lanes)
     mate = spot + 1 - 2 * y
-    token_count, model_width = normed.shape
+    token_count, model_width = resid.shape
     quarter = model_width // lanes
     half = model_width // 2
     span = rows.shape[1]
+    strip = 16
+    tall = 64
     given = (normed, cots)
     laid = (rows, row_cots)
 
@@ -254,12 +258,12 @@
 
     def home(block):
         return remote(
-            summed.at[block], returned.at[spot], send_h.at[block], recv_h.at[spot], sp=block
+            from_far.at[block], returned.at[spot], send_h.at[block], recv_h.at[spot], sp=block
         )
 
     def home_from(block):
         return remote(
-            summed.at[block], returned.at[block], send_h.at[block], recv_h.at[block], sp=block
+            from_far.at[block], returned.at[block], send_h.at[block], recv_h.at[block], sp=block
         )
 
     def matches(block, expert):
@@ -310,7 +314,20 @@
         return carry
 
     lax.fori_loop(1, groups, tell_all, 0)
-    for k in (0, 1):
+    def shift():
+        return remote(
+            edge, edge_got, send_e.at[0], recv_e.at[0], sp=lax.rem(spot + 1, groups)
+        )
+
+    @pl.when(spot < groups - 1)
+    def _():
+        shift().start()
+
+    @pl.when(spot == 0)
+    def _():
+        edge_got[...] = jnp.zeros_like(edge_got)
+
+    def send_own(k):
         for side in (0, 1):
 
             @pl.when(onward(side))
@@ -321,9 +338,22 @@
                     lambda: hop(k, z, side, True).start(),
                 )
 
+    send_own(1)
+
+    def norm_strip(at, carry):
+        picked = pl.ds(pl.multiple_of(at * strip, strip), strip)
+        wide = resid[picked, :].astype(f32)
+        mean = jnp.sum(wide * wide, axis=1, keepdims=True) * (1.0 / model_width)
+        scale = lax.rsqrt(mean + norm_eps)
+        inverse[picked, :] = scale
+        normed[picked, :] = (wide * scale * gain[...]).astype(bf16)
+        return carry
+
+    lax.fori_loop(0, token_count // strip, norm_strip, 0, unroll=2)
+    send_own(0)
     infos[spot] = info[...]
     mine_there = chosen(spot, mate)
-    for k in (0, 1):
+    for k in (1, 0):
         to_mate_own[k] = placed(mine_there, given[k][:, columns(core, half)])
         over_own(k).start()
     mine_here = chosen(spot, spot)
@@ -431,7 +461,23 @@
 
         each_block(level, share)
 
-    def compute_level(level):
+    def ahead(level, side, line):
+        return jnp.logical_and(
+            jnp.logical_and(level > 0, line == 0), is_end(source(side, level))
+        )
+
+    def work_level(level, first):
+        def chosen_now(block, side, line, body):
+            now = ahead(level, side, line)
+
+            @pl.when(now if first else jnp.logical_not(now))
+            def _():
+                body(block, side, line)
+
+        compute_level(level, chosen_now)
+        middle_level(level, chosen_now)
+
+    def compute_level(level, chosen_now):
         def compute(block, side, line):
             @pl.when(level > 0)
             def _():
@@ -489,9 +535,9 @@
             to_core(block, 1).start()
             to_core(block, 0).start()
 
-        each_block(level, compute)
-
-    def middle_level(level):
+        each_block(level, lambda *at: chosen_now(*at, compute))
+
+    def middle_level(level, chosen_now):
         def middle(block, side, line):
             to_core(block, 1).wait_recv()
             to_far[block] = (
@@ -500,7 +546,7 @@
             ).astype(bf16)
             to_far_peer(block).start()
 
-        each_block(level, middle)
+        each_block(level, lambda *at: chosen_now(*at, middle))
 
     def total_level(level):
         def total(block, side, line):
@@ -518,14 +564,20 @@
 
             @pl.when(block != spot)
             def _():
-                summed[block] = value
+                from_far[block] = value
                 home(block).start()
 
         each_block(level, total)
 
-    def weight_grads():
-        slots = groups * span
-        down_in = (((0,), (0,)), ((), ()))
+    slots = groups * span
+    down_in = (((0,), (0,)), ((), ()))
+    grad_copies = [
+        pltpu.make_async_copy(grad_b, down_out, local_sem.at[0]),
+        pltpu.make_async_copy(grad_a.at[0], gate_out, local_sem.at[1]),
+        pltpu.make_async_copy(grad_a.at[1], up_out, local_sem.at[2]),
+    ]
+
+    def down_grad():
 
         def down_step(at, carry):
             picked = columns(at, quarter)
@@ -538,27 +590,21 @@
             return carry
 
         lax.fori_loop(0, lanes, down_step, 0)
-        down_copy = pltpu.make_async_copy(grad_b, down_out, local_sem.at[0])
-        down_copy.start()
-        copies = [down_copy]
-        for spread, out, index in ((dgate, gate_out, 0), (dup, up_out, 1)):
-
-            def step(at, carry):
-                picked = columns(at, quarter)
-                grad_a[index, picked, :] = lax.dot_general(
-                    rows[:, :, picked].reshape(slots, quarter),
-                    spread[...].reshape(slots, spread.shape[2]),
-                    down_in,
-                    preferred_element_type=f32,
-                )
-                return carry
-
-            lax.fori_loop(0, lanes, step, 0)
-            copy = pltpu.make_async_copy(grad_a.at[index], out, local_sem.at[index + 1])
-            copy.start()
-            copies.append(copy)
-        for copy in copies:
-            copy.wait()
+        grad_copies[0].start()
+
+    def wide_grad(spread, index):
+        def step(at, carry):
+            picked = columns(at, quarter)
+            grad_a[index, picked, :] = lax.dot_general(
+                rows[:, :, picked].reshape(slots, quarter),
+                spread[...].reshape(slots, spread.shape[2]),
+                down_in,
+                preferred_element_type=f32,
+            )
+            return carry
+
+        lax.fori_loop(0, lanes, step, 0)
+        grad_copies[index + 1].start()
 
     def advance(level, carry):
         @pl.when(level == 1)
@@ -569,27 +615,29 @@
 
             lax.fori_loop(1, groups, hear_all, 0)
 
+        take_narrow(level, 1)
         take_narrow(level, 0)
-        take_narrow(level, 1)
+        take_wide(level, 1)
+        share_level(level - 1)
+        move_early(level, 0)
+        work_level(level - 1, False)
         take_wide(level, 0)
-        share_level(level - 1)
-        move_early(level, 1)
-        compute_level(level - 1)
-        middle_level(level - 1)
-        take_wide(level, 1)
-        move_early(level + 1, 0)
-        receive_level(level, 0)
+        move_early(level + 1, 1)
+        work_level(level, True)
+        receive_level(level, 1)
 
         @pl.when(level < depth)
         def _():
             total_level(level - 1)
 
-        receive_level(level, 1)
+        receive_level(level, 0)
         return carry
 
     lax.fori_loop(0, depth + 1, advance, 0)
-    weight_grads()
+    down_grad()
     total_level(depth - 1)
+    wide_grad(dgate, 0)
+    wide_grad(dup, 1)
     combined[...] = jnp.zeros_like(combined)
 
     def combine_level(level, carry):
@@ -619,11 +667,57 @@
     gathered[:, columns(lane, quarter)] = combined[...].astype(bf16)
     gather_copy(0, lane, far_peer).start()
     gather_copy(1, lane, core_peer).start()
+    product[...] = jnp.zeros_like(product)
+
+    def add_product(who):
+        wide = columns(who, quarter)
+
+        def step(at, carry):
+            picked = pl.ds(pl.multiple_of(at * tall, tall), tall)
+            pulled = gathered[picked, wide].astype(f32) * gain[:, wide]
+            product[picked, :] += jnp.sum(
+                pulled * resid[picked, wide].astype(f32), axis=1, keepdims=True
+            )
+            return carry
+
+        lax.fori_loop(0, token_count // tall, step, 0)
+
+    add_product(lane)
+    gather_copy(1, lane, core_peer).wait_recv()
+    add_product(core_peer)
     gather_copy(0, lane, far_peer).wait_recv()
     gather_copy(2, far_peer, core_peer).start()
+    add_product(far_peer)
+    gather_copy(2, far_peer, core_peer).wait_recv()
+    add_product(lax.rem(core_peer + lanes // 2, lanes))
+
+    def resid_strip(at, carry):
+        picked = pl.ds(pl.multiple_of(at * strip, strip), strip)
+        scale = inverse[picked, :]
+        pulled = gathered[picked, :].astype(f32) * gain[...]
+        shift_back = scale * scale * scale * (product[picked, :] * (1.0 / model_width))
+        resid_grad[picked, :] = (
+            cots[picked, :].astype(f32)
+            + scale * pulled
+            - resid[picked, :].astype(f32) * shift_back
+        ).astype(bf16)
+        return carry
+
+    lax.fori_loop(0, token_count // strip, resid_strip, 0, unroll=2)
     gather_copy(0, lane, far_peer).wait_send()
-    gather_copy(1, lane, core_peer).wait()
-    gather_copy(2, far_peer, core_peer).wait()
+    gather_copy(1, lane, core_peer).wait_send()
+    gather_copy(2, far_peer, core_peer).wait_send()
+
+    @pl.when(spot < groups - 1)
+    def _():
+        shift().wait_send()
+
+    @pl.when(spot > 0)
+    def _():
+        shift().wait_recv()
+
+    for copy in grad_copies:
+        copy.wait()
 
     def finish_info(offset, carry):
         tell(offset).wait_send()
@@ -686,8 +780,10 @@
     lax.fori_loop(-1, depth, finish_level, 0)
 
 
-def experts(normed, cots, info, targets, gate_mat, up_mat, down_mat, groups, lanes, span):
-    token_count, model_width = normed.shape
+def experts(
+    resid, cots, gain, edge, info, targets, gate_mat, up_mat, down_mat, groups, lanes, span
+):
+    token_count, model_width = resid.shape
     inner = gate_mat.shape[1]
     quarter = model_width // lanes
     width = 2
@@ -703,14 +799,19 @@
     return pl.pallas_call(
         functools.partial(expert_kernel, groups, width, lanes),
         out_shape=(
-            jax.ShapeDtypeStruct(normed.shape, bf16),
+            jax.ShapeDtypeStruct(resid.shape, bf16),
+            jax.ShapeDtypeStruct(edge.shape, f32),
             jax.ShapeDtypeStruct(gate_mat.shape, f32),
             jax.ShapeDtypeStruct(up_mat.shape, f32),
             jax.ShapeDtypeStruct(down_mat.shape, f32),
         ),
-        in_specs=[inside] * 7,
-        out_specs=(inside, anywhere, anywhere, anywhere),
+        in_specs=[inside] * 9,
+        out_specs=(inside, inside, anywhere, anywhere, anywhere),
         scratch_shapes=[
+            vmem(resid.shape, bf16),
+            vmem((token_count, 1), f32),
+            vmem((token_count, 1), f32),
+            vmem(resid.shape, bf16),
             vmem((groups,) + info.shape, f32),
             vmem((2, depth, token_count, quarter), bf16),
             vmem((2, 2, token_count, model_width // 2), bf16),
@@ -724,7 +825,6 @@
             vmem(thin, bf16),
             vmem(whole, bf16),
             vmem((groups, 2, span, quarter), bf16),
-            vmem(block, bf16),
             vmem(block, bf16),
             vmem(block, bf16),
             vmem(block, bf16),
@@ -744,9 +844,10 @@
         + [dma((2, groups))] * 6
         + [dma((groups, 2))] * 2
         + [dma((groups,))] * 4
-        + [dma((3,))] * 2,
+        + [dma((3,))] * 2
+        + [dma((1,))] * 2,
         compiler_params=pltpu.CompilerParams(
-            collective_id=1, has_side_effects=True, vmem_limit_bytes=63 * 2**20
+            collective_id=1, has_side_effects=True, vmem_limit_bytes=67043328
         ),
         cost_estimate=pl.CostEstimate(
             flops=16 * groups * span * model_width * inner,
@@ -754,64 +855,181 @@
             transcendentals=0,
         ),
         name="experts",
-    )(normed, cots, info, targets, gate_mat, up_mat, down_mat)
-
-
-def reduce_kernel(groups, lanes, partial, total, arrived, send_sems, recv_sems):
+    )(resid, cots, gain, edge, info, targets, gate_mat, up_mat, down_mat)
+
+
+def reduce_kernel(
+    groups,
+    width,
+    lanes,
+    partial,
+    edge,
+    total,
+    edge_got,
+    from_mate,
+    sums,
+    arrived,
+    send_y,
+    recv_y,
+    send_z,
+    recv_z,
+    send_e,
+    recv_e,
+):
     f32 = jnp.float32
     spot, lane = lax.axis_index("sp"), lax.axis_index("tp")
+    depth = groups // width
+    z, y = lax.div(spot, width), lax.rem(spot, width)
+    mate = spot + 1 - 2 * y
     core_peer = lane + 1 - 2 * lax.rem(lane, 2)
     far_peer = lax.rem(lane + lanes // 2, lanes)
 
-    def across(offset):
-        goal = lax.rem(spot + offset, groups)
-        return remote(
-            partial.at[goal],
-            arrived.at[offset],
-            send_sems.at[offset],
-            recv_sems.at[offset],
-            sp=goal,
-        )
+    def goal_of(step):
+        return lax.rem(z + step + 1, depth)
+
+    def over(at):
+        return remote(
+            partial.at[at * width + 1 - y],
+            from_mate.at[at],
+            send_y.at[at],
+            recv_y.at[at],
+            sp=mate,
+        )
+
+    def along(at):
+        return remote(
+            sums.at[at], arrived.at[z], send_z.at[at], recv_z.at[z], sp=at * width + y
+        )
+
+    def along_from(at):
+        return remote(
+            sums.at[at], arrived.at[at], send_z.at[at], recv_z.at[at], sp=at * width + y
+        )
+
+    def shift():
+        goal = lax.rem(spot + groups - 1, groups)
+        return remote(edge, edge_got, send_e.at[0], recv_e.at[0], sp=goal)
 
     greet(groups, spot, core_peer, far_peer)
 
-    def launch(offset, carry):
-        across(offset).start()
-        return carry
-
-    lax.fori_loop(1, groups, launch, 0)
-    total[...] = partial[spot].astype(f32)
-
-    def add(offset, carry):
-        across(offset).wait_recv()
-        total[...] += arrived[offset].astype(f32)
-        return carry
-
-    lax.fori_loop(1, groups, add, 0)
-
-    def finish(offset, carry):
-        across(offset).wait_send()
-        return carry
-
-    lax.fori_loop(1, groups, finish, 0)
-
-
-def reduce_rows(partial, groups, lanes):
-    sem = pltpu.SemaphoreType.DMA
+    @pl.when(spot > 0)
+    def _():
+        shift().start()
+
+    @pl.when(spot == groups - 1)
+    def _():
+        edge_got[...] = jnp.zeros_like(edge_got)
+
+    def launch(step, carry):
+        over(goal_of(step)).start()
+        return carry
+
+    lax.fori_loop(0, depth, launch, 0)
+
+    def pair(step, carry):
+        at = goal_of(step)
+        over(at).wait_recv()
+        both = partial[at * width + y].astype(f32) + from_mate[at].astype(f32)
+
+        @pl.when(at == z)
+        def _():
+            total[...] = both
+
+        @pl.when(at != z)
+        def _():
+            sums[at] = both.astype(sums.dtype)
+            along(at).start()
+
+        return carry
+
+    lax.fori_loop(0, depth, pair, 0)
+
+    def add(step, carry):
+        at = lax.rem(z + depth - 1 - step, depth)
+        along_from(at).wait_recv()
+        total[...] += arrived[at].astype(f32)
+        return carry
+
+    lax.fori_loop(0, depth - 1, add, 0)
+
+    def finish(step, carry):
+        at = goal_of(step)
+        over(at).wait_send()
+
+        @pl.when(at != z)
+        def _():
+            along(at).wait_send()
+
+        return carry
+
+    lax.fori_loop(0, depth, finish, 0)
+
+    @pl.when(spot > 0)
+    def _():
+        shift().wait_send()
+
+    @pl.when(spot < groups - 1)
+    def _():
+        shift().wait_recv()
+
+
+def reduce_rows(partial, edge, groups, lanes):
+    width = 2
+    depth = groups // width
+    dma = pltpu.SemaphoreType.DMA
     inside = pl.BlockSpec(memory_space=pltpu.VMEM)
+    held = pltpu.VMEM((depth,) + partial.shape[1:], partial.dtype)
     return pl.pallas_call(
-        functools.partial(reduce_kernel, groups, lanes),
-        out_shape=jax.ShapeDtypeStruct(partial.shape[1:], jnp.float32),
-        in_specs=[inside],
-        out_specs=inside,
-        scratch_shapes=[
-            pltpu.VMEM(partial.shape, partial.dtype),
-            sem((groups,)),
-            sem((groups,)),
-        ],
+        functools.partial(reduce_kernel, groups, width, lanes),
+        out_shape=(
+            jax.ShapeDtypeStruct(partial.shape[1:], jnp.float32),
+            jax.ShapeDtypeStruct(edge.shape, edge.dtype),
+        ),
+        in_specs=[inside] * 2,
+        out_specs=(inside, inside),
+        scratch_shapes=[held] * 3 + [dma((depth,))] * 4 + [dma((1,))] * 2,
         compiler_params=pltpu.CompilerParams(collective_id=4, has_side_effects=True),
         name="reduce_rows",
-    )(partial)
+    )(partial, edge)
+
+
+def hand_kernel(count, parts, *refs):
+    given, out, held = refs[:count], refs[count : 2 * count], refs[2 * count : 3 * count]
+    come, go = refs[3 * count :]
+
+    def piece(ref, at):
+        step = ref.shape[0] // parts
+        return ref.at[at * step : (at + 1) * step]
+
+    def inward(k, at):
+        return pltpu.make_async_copy(piece(given[k], at), piece(held[k], at), come.at[k, at])
+
+    def outward(k, at):
+        return pltpu.make_async_copy(piece(held[k], at), piece(out[k], at), go.at[k, at])
+
+    every = [(k, at) for k in range(count) for at in range(parts)]
+    for k, at in every:
+        inward(k, at).start()
+    for k, at in every:
+        inward(k, at).wait()
+        outward(k, at).start()
+    for k, at in every:
+        outward(k, at).wait()
+
+
+def hand_over(*arrays):
+    parts = 2
+    count = len(arrays)
+    anywhere = pl.BlockSpec(memory_space=pl.ANY)
+    dma = pltpu.SemaphoreType.DMA((count, parts))
+    return pl.pallas_call(
+        functools.partial(hand_kernel, count, parts),
+        out_shape=tuple(jax.ShapeDtypeStruct(a.shape, a.dtype) for a in arrays),
+        in_specs=[anywhere] * count,
+        out_specs=(anywhere,) * count,
+        scratch_shapes=[pltpu.VMEM(a.shape, a.dtype) for a in arrays] + [dma, dma],
+        name="hand_over",
+    )(*arrays)
 
 
 def on_device(
@@ -838,11 +1056,6 @@
     expert_total = local_experts * groups
     capacity = 4 * token_count // expert_total
     slot_span = local_experts * capacity
-    resid_wide = resid_in.astype(f32)
-    inv_rms = lax.rsqrt(jnp.mean(resid_wide * resid_wide, axis=1, keepdims=True) + norm_eps)
-    normed = (resid_wide * inv_rms * norm_gain).astype(bf16)
-    mixed = gate_c.astype(f32) * values_u.astype(f32)
-    earlier = passed_along(mixed[-2:], "sp", 1)
     names = jnp.arange(expert_total, dtype=jnp.int32)
     chosen = routes[:, :, None] == names[None, None, :]
     named = jnp.any(chosen, axis=1).astype(bf16)
@@ -859,9 +1072,12 @@
         ],
         axis=0,
     )
-    gathered, grad_gate, grad_up, grad_down = experts(
-        normed,
+    edge = gate_c[-8:].astype(f32) * values_u[-8:].astype(f32)
+    grad_resid, earlier, grad_gate, grad_up, grad_down = experts(
+        resid_in,
         cotangent,
+        norm_gain[None, :],
+        edge,
         info,
         targets.astype(f32),
         gate_weight[0],
@@ -871,15 +1087,8 @@
         lanes,
         slot_span,
     )
-    dnormed = gathered.astype(f32)
-    scaled = dnormed * norm_gain
-    resid_grad = (
-        cotangent.astype(f32)
-        + inv_rms * scaled
-        - resid_wide * inv_rms**3 * jnp.mean(scaled * resid_wide, axis=1, keepdims=True)
-    )
-    grad_resid = resid_grad.astype(bf16)
-    extended = jnp.concatenate([earlier, mixed], axis=0)
+    mixed = gate_c.astype(f32) * values_u.astype(f32)
+    extended = jnp.concatenate([earlier[-2:], mixed], axis=0)
     conv = (
         taps[0] * extended[:token_count]
         + taps[1] * extended[1 : token_count + 1]
@@ -887,16 +1096,16 @@
     )
     merged = (gate_b.astype(f32) * conv).astype(bf16)
     out_partial = jnp.einsum("td,tc->dc", grad_resid, merged, preferred_element_type=f32)
-    grad_out_weight = reduce_rows(
+    dmerged = jnp.dot(grad_resid, out_weight, preferred_element_type=f32)
+    grad_gate_b = (dmerged * conv).astype(bf16)
+    dconv = dmerged * gate_b.astype(f32)
+    grad_out_weight, later = reduce_rows(
         out_partial.astype(bf16).reshape(groups, model_width // groups, merged.shape[1]),
+        dconv[:8],
         groups,
         lanes,
     )
-    dmerged = jnp.dot(grad_resid, out_weight, preferred_element_type=f32)
-    grad_gate_b = (dmerged * conv).astype(bf16)
-    dconv = dmerged * gate_b.astype(f32)
-    later = passed_along(dconv[:2], "sp", -1)
-    extended_grad = jnp.concatenate([dconv, later], axis=0)
+    extended_grad = jnp.concatenate([dconv, later[:2]], axis=0)
     dmixed = (
         taps[2] * extended_grad[:token_count]
         + taps[1] * extended_grad[1 : token_count + 1]
@@ -904,11 +1113,14 @@
     )
     grad_gate_c = (dmixed * values_u.astype(f32)).astype(bf16)
     grad_values = (dmixed * gate_c.astype(f32)).astype(bf16)
+    grad_gate, grad_up, grad_down, grad_resid_out, grad_out_weight = hand_over(
+        grad_gate, grad_up, grad_down, grad_resid, grad_out_weight
+    )
     return (
         grad_gate[None],
         grad_up[None],
         grad_down[None],
-        grad_resid,
+        grad_resid_out,
         grad_out_weight,
         grad_gate_b,
         grad_gate_c,

time: 193 us -> 185 us (0.959); the launches traced: 193 us -> 182 us
  starting transfers between devices: 6.4 us -> 0 us
  other arithmetic: 12.7 us -> 8.14 us
  local copies, waits for them, and re-layouts: 7.26 us -> 3.13 us
  Pallas kernels: 162 us -> 165 us
    pallas_call x1 -> x2, Pallas kernels: 33.3 us -> 41.3 us  [the longest x1 35.1 us: reduce_rows(): pl.pallas_call(functools.partial(reduce_kernel, groups, width, lanes), ou...]
    unnamed x36 -> x8, local copies, waits for them, and re-layouts: 6.95 us -> 0.02 us
    ppermute x2 -> x0, starting transfers between devices: 6.4 us -> none  [passed_along(): return lax.ppermute(array, axis, pairs)]
    pallas_call x1, Pallas kernels: 129 us -> 124 us  [experts(): pl.pallas_call(functools.partial(expert_kernel, groups, width, lanes), ou...]
    reduce_sum x2 -> x0, other arithmetic: 4.41 us -> none  [the longest x1 2.62 us: on_device(): jnp.mean(scaled * resid_wide, axis=1, keepdims=True)]
    convert_element_type x2 -> x0, other arithmetic: 4.12 us -> none  [the longest x1 2.53 us: on_device(): grad_resid = resid_grad.astype(bf16)]
    slice x2 -> x3, local copies, waits for them, and re-layouts: 0.01 us -> 2 us  [the longest x1 0.7 us: on_device(): extended = jnp.concatenate([earlier[-2:], mixed], axis=0)]
  transfers between devices with their start and end apart: 2 -> 0, of which waited for: 0 -> 0; matrix products, arithmetic and copies ran while one was open for 6% -> 0% of each run, Pallas kernels for 84% -> 0%
where the time goes in v3:
time: 185 us; the launch traced here: 182 us
  Pallas kernels  165 us (89%)
  other arithmetic  8.14 us (4%)
  matrix products  5 us (3%)
  local copies, waits for them, and re-layouts  3.13 us (2%)
    pallas_call x1, Pallas kernels, experts(): pl.pallas_call(functools.partial(expert_kernel, groups, width, lanes), ou...  124 us
    pallas_call x1, Pallas kernels, reduce_rows(): pl.pallas_call(functools.partial(reduce_kernel, groups, width, lanes), ou...  35.1 us
    pallas_call x1, Pallas kernels, hand_over(): pl.pallas_call(functools.partial(hand_kernel, count, parts), out_shape=tu...  6.26 us

profile of v3, /device:TPU:12, one launch (start us, length us, event | category | flops | bytes accessed | tf_op | source)
XLA Modules:
  0.0 182.0 jit_solution(16566845469039385115)
XLA Ops:
  0.6 0.7 fusion.14
  1.3 0.1 convolution_convert_fusion.1
  1.5 0.8 select_reduce_fusion
  2.2 0.7 multiply_add_fusion
  2.9 0.1 copy.31
  3.1 0.7 fusion.17
  3.8 0.1 copy.32
  3.9 0.1 pad.6.clone
  4.0 1.4 maximum_maximum_fusion.info
  5.3 1.3 convert_multiply_fusion.5.edge
  6.6 123.7 %experts.1 = (bf16[384,2048]{1,0:T(8,128)(2,1)}, f32[8,256]{1,0:T(8,128)}, f32[2048,256]{1,0:T(8,128)}, f32[2048,256]{1,0:T(8,128)}, f32[256,2048]{1,0:T(8,128)}) custom-call(bf16[384,2048]{1,0:T(8,128)(2,1)} %resid.1, bf16[384,2048]{1,0:T(8,128)(2,1)} %cots.1, f32[1,2048]{1,0:T(1,128)} %bitcast.32, f32[8,256]{1,0:T(8,128)} %convert_multiply_fusion.5.edge, ...), custom_call_target="tpu_custom_call" | custom-call | flops 12884901888 | bytes 157286400 | tf_op jit(solution)/shard_map/experts/pallas_call | solution.py:799
  130.3 0.7 slice.42
  131.0 0.8 fusion.18
  131.8 1.1 convert_multiply_fusion.1
  132.9 0.0 copy-start.3
  132.9 3.1 %multiply_convert_fusion = (bf16[384,256]{1,0:T(8,128)(2,1)}, f32[384,256]{1,0:T(8,128)S(1)}, f32[384,256]{1,0:T(8,128)S(1)}) fusion(f32[384,256]{1,0:T(8,128)S(1)} %convert_multiply_fusion.1, f32[256]{0:T(256)S(1)} %bitcast.21, f32[2,256]{1,0:T(2,128)S(1)} %slice.42, f32[256]{0:T(256)S(1)} %bitcast.23, f32[256]{0:T(256)S(1)} %bitcast.19, ...), kind=kOutput, calls=%fused_computation.27 | convolution fusion | flops 403734528 | bytes 4199424 | tf_op jit(solution)/shard_map/dot_general | solution.py:1099
  136.0 1.7 convolution_convert_fusion
  137.8 0.6 slice.53.edge
  138.4 35.1 %reduce_rows.1 = (f32[256,256]{1,0:T(8,128)}, f32[8,256]{1,0:T(8,128)}) custom-call(bf16[8,256,256]{2,1,0:T(8,128)(2,1)} %bitcast.18, f32[8,256]{1,0:T(8,128)} %slice.53.edge), custom_call_target="tpu_custom_call" | custom-call | tf_op jit(solution)/shard_map/reduce_rows/pallas_call | solution.py:982
  173.5 0.7 slice.48
  174.2 0.0 copy-done.2
  174.2 0.8 fusion.9
  175.0 0.7 fusion.10
  175.7 6.3 %hand_over.1 = (f32[2048,256]{1,0:T(8,128)}, f32[2048,256]{1,0:T(8,128)}, f32[256,2048]{1,0:T(8,128)}, bf16[384,2048]{1,0:T(8,128)(2,1)}, f32[256,256]{1,0:T(8,128)}) custom-call(f32[2048,256]{1,0:T(8,128)} %get-tuple-element.20.refs_0_, f32[2048,256]{1,0:T(8,128)} %get-tuple-element.21.refs_1_, f32[256,2048]{1,0:T(8,128)} %get-tuple-element.22.refs_2_, ...), custom_call_target="tpu_custom_call" | custom-call | tf_op jit(solution)/shard_map/hand_over/pallas_call | solution.py:1025
  (7 shorter events, 0.0 us)
Async XLA Ops:
  132.9 3.1 %copy-start = (bf16[384,2048]{1,0:T(8,128)(2,1)S(1)}, bf16[384,2048]{1,0:T(8,128)(2,1)}, u32[]{:S(2)}) copy-start(bf16[384,2048]{1,0:T(8,128)(2,1)} %get-tuple-element.23.refs_3_) | copy-start | bytes 4718596
  132.9 3.1 %copy-start.3 = (bf16[384,256]{1,0:T(8,128)(2,1)S(1)}, bf16[384,256]{1,0:T(8,128)(2,1)}, u32[]{:S(2)}) copy-start(bf16[384,256]{1,0:T(8,128)(2,1)} %param.22) | copy-start | bytes 589828
  136.0 38.1 %copy-start.2 = (bf16[384,256]{1,0:T(8,128)(2,1)S(1)}, bf16[384,256]{1,0:T(8,128)(2,1)}, u32[]{:S(2)}) copy-start(bf16[384,256]{1,0:T(8,128)(2,1)} %param.23) | copy-start | bytes 589828
  137.8 37.2 %copy-start.1 = (bf16[384,256]{1,0:T(8,128)(2,1)S(1)}, bf16[384,256]{1,0:T(8,128)(2,1)}, u32[]{:S(2)}) copy-start(bf16[384,256]{1,0:T(8,128)(2,1)} %param.24) | copy-start | bytes 589828

commit v4 on v3

--- a/solution.py
+++ b/solution.py
@@ -38,7 +38,7 @@
         pl.semaphore_signal(
             barrier, inc=1, device_id={"tp": peer}, device_id_type=pl.DeviceIdType.MESH
         )
-    pl.semaphore_wait(barrier, groups + 1)
+    return lambda: pl.semaphore_wait(barrier, groups + 1)
 
 
 def expert_kernel(
@@ -48,9 +48,10 @@
     resid,
     cots,
     gain,
-    edge,
-    info,
-    targets,
+    gate_c,
+    values_u,
+    routes,
+    route_weights,
     gate_mat,
     up_mat,
     down_mat,
@@ -63,6 +64,7 @@
     inverse,
     product,
     gathered,
+    edge,
     infos,
     dense,
     dense_wide,
@@ -153,11 +155,11 @@
 
     def tell(offset):
         goal = lax.rem(spot + offset, groups)
-        return remote(info, infos.at[spot], send_i.at[offset], recv_i.at[spot], sp=goal)
+        return remote(infos.at[spot], infos.at[spot], send_i.at[offset], recv_i.at[spot], sp=goal)
 
     def told(offset):
         origin = lax.rem(spot - offset + groups, groups)
-        return remote(info, infos.at[origin], send_i.at[offset], recv_i.at[origin], sp=origin)
+        return remote(infos.at[origin], infos.at[origin], send_i.at[offset], recv_i.at[origin], sp=origin)
 
     def is_end(at):
         return jnp.logical_or(at == 0, at == depth - 1)
@@ -306,8 +308,27 @@
 
         lax.fori_loop(0, 4, step, 0)
 
-    core_side, far_side = core_peer, far_peer
-    greet(groups, spot, core_side, far_side)
+    all_here = greet(groups, spot, core_peer, far_peer)
+    last = edge.shape[0]
+    edge[...] = gate_c[token_count - last :, :].astype(f32) * values_u[
+        token_count - last :, :
+    ].astype(f32)
+    named = lax.broadcasted_iota(jnp.int32, (groups, token_count), 0)
+    picks = [named == routes[at : at + 1, :] for at in (0, 1)]
+    counted = jnp.where(jnp.logical_or(picks[0], picks[1]), 1.0, 0.0).astype(bf16)
+    square = (token_count, token_count)
+    strict = jnp.where(
+        lax.broadcasted_iota(jnp.int32, square, 0) < lax.broadcasted_iota(jnp.int32, square, 1),
+        1.0,
+        0.0,
+    ).astype(bf16)
+    before = jnp.dot(counted, strict, preferred_element_type=f32)
+    for at in (0, 1):
+        rank = jnp.sum(jnp.where(picks[at], before, 0.0), axis=0, keepdims=True)
+        first_slot = (routes[at : at + 1, :] * span).astype(f32)
+        infos[spot, at : at + 1, :] = first_slot + rank
+        infos[spot, at + 2 : at + 3, :] = route_weights[at : at + 1, :]
+    all_here()
 
     def tell_all(offset, carry):
         tell(offset).start()
@@ -351,7 +372,6 @@
 
     lax.fori_loop(0, token_count // strip, norm_strip, 0, unroll=2)
     send_own(0)
-    infos[spot] = info[...]
     mine_there = chosen(spot, mate)
     for k in (1, 0):
         to_mate_own[k] = placed(mine_there, given[k][:, columns(core, half)])
@@ -646,11 +666,9 @@
             def _():
                 home_from(block).wait_recv()
 
-            slot = lax.broadcasted_iota(jnp.int32, (token_count, span), 1) + block * span
-            slot = slot.astype(f32)
-            hit = jnp.logical_or(slot == targets[:, 0:1], slot == targets[:, 1:2])
-            picked = jnp.where(hit, 1.0, 0.0).astype(bf16)
-            combined[...] += jnp.dot(picked, returned[block], preferred_element_type=f32)
+            combined[...] += lax.dot_general(
+                chosen(spot, block), returned[block], down_in, preferred_element_type=f32
+            )
 
         each_block(level, combine)
         return carry
@@ -781,7 +799,19 @@
 
 
 def experts(
-    resid, cots, gain, edge, info, targets, gate_mat, up_mat, down_mat, groups, lanes, span
+    resid,
+    cots,
+    gain,
+    gate_c,
+    values_u,
+    routes,
+    route_weights,
+    gate_mat,
+    up_mat,
+    down_mat,
+    groups,
+    lanes,
+    span,
 ):
     token_count, model_width = resid.shape
     inner = gate_mat.shape[1]
@@ -795,24 +825,26 @@
     block = (groups, span, quarter)
     whole = (groups, span, model_width)
     thin = (groups, span, inner)
+    edge_shape = (16, gate_c.shape[1])
     vmem = pltpu.VMEM
     return pl.pallas_call(
         functools.partial(expert_kernel, groups, width, lanes),
         out_shape=(
             jax.ShapeDtypeStruct(resid.shape, bf16),
-            jax.ShapeDtypeStruct(edge.shape, f32),
+            jax.ShapeDtypeStruct(edge_shape, f32),
             jax.ShapeDtypeStruct(gate_mat.shape, f32),
             jax.ShapeDtypeStruct(up_mat.shape, f32),
             jax.ShapeDtypeStruct(down_mat.shape, f32),
         ),
-        in_specs=[inside] * 9,
+        in_specs=[inside] * 10,
         out_specs=(inside, inside, anywhere, anywhere, anywhere),
         scratch_shapes=[
             vmem(resid.shape, bf16),
             vmem((token_count, 1), f32),
             vmem((token_count, 1), f32),
             vmem(resid.shape, bf16),
-            vmem((groups,) + info.shape, f32),
+            vmem(edge_shape, f32),
+            vmem((groups, 8, token_count), f32),
             vmem((2, depth, token_count, quarter), bf16),
             vmem((2, 2, token_count, model_width // 2), bf16),
             vmem((2, depth, span, quarter), bf16),
@@ -855,16 +887,42 @@
             transcendentals=0,
         ),
         name="experts",
-    )(resid, cots, gain, edge, info, targets, gate_mat, up_mat, down_mat)
-
-
-def reduce_kernel(
+    )(
+        resid,
+        cots,
+        gain,
+        gate_c,
+        values_u,
+        routes,
+        route_weights,
+        gate_mat,
+        up_mat,
+        down_mat,
+    )
+
+
+def tail_kernel(
     groups,
     width,
     lanes,
+    pieces,
+    resid_grad,
+    earlier,
+    out_mat,
+    gate_b,
+    gate_c,
+    values_u,
+    taps,
+    total,
+    grad_b,
+    grad_c,
+    grad_u,
     partial,
+    mixed,
+    conv,
+    merged,
+    pulled,
     edge,
-    total,
     edge_got,
     from_mate,
     sums,
@@ -877,12 +935,17 @@
     recv_e,
 ):
     f32 = jnp.float32
+    bf16 = jnp.bfloat16
     spot, lane = lax.axis_index("sp"), lax.axis_index("tp")
     depth = groups // width
     z, y = lax.div(spot, width), lax.rem(spot, width)
     mate = spot + 1 - 2 * y
     core_peer = lane + 1 - 2 * lax.rem(lane, 2)
     far_peer = lax.rem(lane + lanes // 2, lanes)
+    token_count, model_width = resid_grad.shape
+    piece = model_width // pieces
+    per = depth // pieces
+    lead = earlier.shape[0]
 
     def goal_of(step):
         return lax.rem(z + step + 1, depth)
@@ -910,7 +973,48 @@
         goal = lax.rem(spot + groups - 1, groups)
         return remote(edge, edge_got, send_e.at[0], recv_e.at[0], sp=goal)
 
-    greet(groups, spot, core_peer, far_peer)
+    all_here = greet(groups, spot, core_peer, far_peer)
+    mixed[0:lead, :] = earlier[...]
+    mixed[lead:, :] = gate_c[...].astype(f32) * values_u[...].astype(f32)
+    conv[...] = (
+        taps[0:1, :] * mixed[lead - 2 : lead - 2 + token_count, :]
+        + taps[1:2, :] * mixed[lead - 1 : lead - 1 + token_count, :]
+        + taps[2:3, :] * mixed[lead : lead + token_count, :]
+    )
+    merged[...] = (gate_b[...].astype(f32) * conv[...]).astype(bf16)
+
+    def make(step):
+        at = lax.rem(lax.div(z, per) + step + 1, pieces)
+        made = lax.dot_general(
+            resid_grad[:, pl.ds(pl.multiple_of(at * piece, piece), piece)],
+            merged[...],
+            (((0,), (0,)), ((), ())),
+            preferred_element_type=f32,
+        ).astype(bf16)
+        count = per * width
+        partial[pl.ds(at * count, count)] = made.reshape((count,) + partial.shape[1:])
+        return at
+
+    first = make(0)
+    all_here()
+
+    def launch(at):
+        def step(k, carry):
+            over(at * per + k).start()
+            return carry
+
+        lax.fori_loop(0, per, step, 0)
+
+    launch(first)
+
+    def make_next(step, carry):
+        launch(make(step))
+        return carry
+
+    lax.fori_loop(1, pieces, make_next, 0)
+    dmerged = jnp.dot(resid_grad[...], out_mat[...], preferred_element_type=f32)
+    pulled[0:token_count, :] = dmerged * gate_b[...].astype(f32)
+    edge[...] = pulled[0 : edge.shape[0], :]
 
     @pl.when(spot > 0)
     def _():
@@ -920,11 +1024,7 @@
     def _():
         edge_got[...] = jnp.zeros_like(edge_got)
 
-    def launch(step, carry):
-        over(goal_of(step)).start()
-        return carry
-
-    lax.fori_loop(0, depth, launch, 0)
+    grad_b[...] = (dmerged * conv[...]).astype(bf16)
 
     def pair(step, carry):
         at = goal_of(step)
@@ -943,6 +1043,19 @@
         return carry
 
     lax.fori_loop(0, depth, pair, 0)
+
+    @pl.when(spot < groups - 1)
+    def _():
+        shift().wait_recv()
+
+    pulled[token_count:, :] = edge_got[...]
+    dmixed = (
+        taps[2:3, :] * pulled[0:token_count, :]
+        + taps[1:2, :] * pulled[1 : token_count + 1, :]
+        + taps[0:1, :] * pulled[2 : token_count + 2, :]
+    )
+    grad_c[...] = (dmixed * values_u[...].astype(f32)).astype(bf16)
+    grad_u[...] = (dmixed * gate_c[...].astype(f32)).astype(bf16)
 
     def add(step, carry):
         at = lax.rem(z + depth - 1 - step, depth)
@@ -968,29 +1081,46 @@
     def _():
         shift().wait_send()
 
-    @pl.when(spot < groups - 1)
-    def _():
-        shift().wait_recv()
-
-
-def reduce_rows(partial, edge, groups, lanes):
+
+def tail(resid_grad, earlier, out_mat, gate_b, gate_c, values_u, taps, groups, lanes):
     width = 2
     depth = groups // width
+    pieces = lanes if depth % lanes == 0 else 1
+    token_count, model_width = resid_grad.shape
+    channels = out_mat.shape[1]
+    bf16, f32 = jnp.bfloat16, jnp.float32
     dma = pltpu.SemaphoreType.DMA
-    inside = pl.BlockSpec(memory_space=pltpu.VMEM)
-    held = pltpu.VMEM((depth,) + partial.shape[1:], partial.dtype)
+    vmem = pltpu.VMEM
+    inside = pl.BlockSpec(memory_space=vmem)
+    block = (model_width // groups, channels)
+    flat = (token_count, channels)
+    edge_shape = (8, channels)
+    held = vmem((depth,) + block, bf16)
     return pl.pallas_call(
-        functools.partial(reduce_kernel, groups, width, lanes),
-        out_shape=(
-            jax.ShapeDtypeStruct(partial.shape[1:], jnp.float32),
-            jax.ShapeDtypeStruct(edge.shape, edge.dtype),
+        functools.partial(tail_kernel, groups, width, lanes, pieces),
+        out_shape=(jax.ShapeDtypeStruct(block, f32),)
+        + (jax.ShapeDtypeStruct(flat, bf16),) * 3,
+        in_specs=[inside] * 7,
+        out_specs=(inside,) * 4,
+        scratch_shapes=[
+            vmem((groups,) + block, bf16),
+            vmem((token_count + earlier.shape[0], channels), f32),
+            vmem(flat, f32),
+            vmem(flat, bf16),
+            vmem((token_count + 8, channels), f32),
+            vmem(edge_shape, f32),
+            vmem(edge_shape, f32),
+            held,
+            held,
+            held,
+        ]
+        + [dma((depth,))] * 4
+        + [dma((1,))] * 2,
+        compiler_params=pltpu.CompilerParams(
+            collective_id=4, has_side_effects=True, vmem_limit_bytes=67043328
         ),
-        in_specs=[inside] * 2,
-        out_specs=(inside, inside),
-        scratch_shapes=[held] * 3 + [dma((depth,))] * 4 + [dma((1,))] * 2,
-        compiler_params=pltpu.CompilerParams(collective_id=4, has_side_effects=True),
-        name="reduce_rows",
-    )(partial, edge)
+        name="tail",
+    )(resid_grad, earlier, out_mat, gate_b, gate_c, values_u, taps)
 
 
 def hand_kernel(count, parts, *refs):
@@ -1028,6 +1158,7 @@
         in_specs=[anywhere] * count,
         out_specs=(anywhere,) * count,
         scratch_shapes=[pltpu.VMEM(a.shape, a.dtype) for a in arrays] + [dma, dma],
+        compiler_params=pltpu.CompilerParams(vmem_limit_bytes=67043328),
         name="hand_over",
     )(*arrays)
 
@@ -1047,85 +1178,30 @@
     values_u,
     taps,
 ):
-    f32 = jnp.float32
-    bf16 = jnp.bfloat16
-    token_count, model_width = resid_in.shape
     groups = lax.axis_size("sp")
     lanes = lax.axis_size("tp")
-    local_experts = gate_weight.shape[0]
-    expert_total = local_experts * groups
-    capacity = 4 * token_count // expert_total
-    slot_span = local_experts * capacity
-    names = jnp.arange(expert_total, dtype=jnp.int32)
-    chosen = routes[:, :, None] == names[None, None, :]
-    named = jnp.any(chosen, axis=1).astype(bf16)
-    order = jnp.arange(token_count, dtype=jnp.int32)
-    strict = (order[:, None] > order[None, :]).astype(bf16)
-    before = jnp.dot(strict, named, preferred_element_type=f32).astype(jnp.int32)
-    rank = jnp.sum(jnp.where(chosen, before[:, None, :], 0), axis=2)
-    targets = routes * capacity + rank
-    info = jnp.concatenate(
-        [
-            targets.T.astype(f32),
-            route_weights.T,
-            jnp.zeros((4, token_count), f32),
-        ],
-        axis=0,
-    )
-    edge = gate_c[-8:].astype(f32) * values_u[-8:].astype(f32)
+    expert_total = gate_weight.shape[0] * groups
+    capacity = 4 * resid_in.shape[0] // expert_total
     grad_resid, earlier, grad_gate, grad_up, grad_down = experts(
         resid_in,
         cotangent,
         norm_gain[None, :],
-        edge,
-        info,
-        targets.astype(f32),
+        gate_c,
+        values_u,
+        routes.T,
+        route_weights.T,
         gate_weight[0],
         up_weight[0],
         down_weight[0],
         groups,
         lanes,
-        slot_span,
+        gate_weight.shape[0] * capacity,
     )
-    mixed = gate_c.astype(f32) * values_u.astype(f32)
-    extended = jnp.concatenate([earlier[-2:], mixed], axis=0)
-    conv = (
-        taps[0] * extended[:token_count]
-        + taps[1] * extended[1 : token_count + 1]
-        + taps[2] * extended[2 : token_count + 2]
+    given = tail(
+        grad_resid, earlier, out_weight, gate_b, gate_c, values_u, taps, groups, lanes
     )
-    merged = (gate_b.astype(f32) * conv).astype(bf16)
-    out_partial = jnp.einsum("td,tc->dc", grad_resid, merged, preferred_element_type=f32)
-    dmerged = jnp.dot(grad_resid, out_weight, preferred_element_type=f32)
-    grad_gate_b = (dmerged * conv).astype(bf16)
-    dconv = dmerged * gate_b.astype(f32)
-    grad_out_weight, later = reduce_rows(
-        out_partial.astype(bf16).reshape(groups, model_width // groups, merged.shape[1]),
-        dconv[:8],
-        groups,
-        lanes,
-    )
-    extended_grad = jnp.concatenate([dconv, later[:2]], axis=0)
-    dmixed = (
-        taps[2] * extended_grad[:token_count]
-        + taps[1] * extended_grad[1 : token_count + 1]
-        + taps[0] * extended_grad[2 : token_count + 2]
-    )
-    grad_gate_c = (dmixed * values_u.astype(f32)).astype(bf16)
-    grad_values = (dmixed * gate_c.astype(f32)).astype(bf16)
-    grad_gate, grad_up, grad_down, grad_resid_out, grad_out_weight = hand_over(
-        grad_gate, grad_up, grad_down, grad_resid, grad_out_weight
-    )
-    return (
-        grad_gate[None],
-        grad_up[None],
-        grad_down[None],
-        grad_resid_out,
-        grad_out_weight,
-        grad_gate_b,
-        grad_gate_c,
-        grad_values,
-    )
+    results = hand_over(grad_gate, grad_up, grad_down, grad_resid, *given)
+    return tuple(array[None] for array in results[:3]) + tuple(results[3:])
 
 
 def solution(mesh):

time: 185 us -> 169 us (0.914)
  other arithmetic: 8.14 us -> 0 us
  matrix products: 5 us -> 0 us
  local copies, waits for them, and re-layouts: 3.13 us -> 0 us
    dot_general x3 -> x0, matrix products: 5 us -> none  [the longest x1 3.12 us: on_device(): dmerged = jnp.dot(grad_resid, out_weight, preferred_element_type=f32)]
    slice x4 -> x0, local copies, waits for them, and re-layouts: 2.8 us -> none  [the longest x1 0.8 us: on_device(): taps[0] * extended[:token_count] + taps[1] * extended[1:token_count + 1]]
    mul x2 -> x0, other arithmetic: 2.37 us -> none  [the longest x1 1.3 us: on_device(): edge = gate_c[-8:].astype(f32) * values_u[-8:].astype(f32)]
    convert_element_type x3 -> x0, other arithmetic: 2.27 us -> none  [the longest x1 0.83 us: on_device(): grad_values = (dmixed * gate_c.astype(f32)).astype(bf16)]
where the time goes in v4:
time: 169 us; the launch traced here: 167 us
  Pallas kernels  166 us (98%)
    pallas_call x1, Pallas kernels, experts(): pl.pallas_call(functools.partial(expert_kernel, groups, width, lanes), ou...  124 us
    pallas_call x1, Pallas kernels, tail(): pl.pallas_call(functools.partial(tail_kernel, groups, width, lanes, piece...  35.6 us
    pallas_call x1, Pallas kernels, hand_over(): pl.pallas_call(functools.partial(hand_kernel, count, parts), out_shape=tu...  6.56 us

profile of v4, /device:TPU:12, one launch (start us, length us, event | category | flops | bytes accessed | tf_op | source)
XLA Modules:
  0.0 166.9 jit_solution(3998490501491003995)
XLA Ops:
  0.6 124.1 %experts.1 = (bf16[384,2048]{1,0:T(8,128)(2,1)}, f32[16,256]{1,0:T(8,128)}, f32[2048,256]{1,0:T(8,128)}, f32[2048,256]{1,0:T(8,128)}, f32[256,2048]{1,0:T(8,128)}) custom-call(bf16[384,2048]{1,0:T(8,128)(2,1)} %resid.1, bf16[384,2048]{1,0:T(8,128)(2,1)} %cots.1, f32[1,2048]{1,0:T(1,128)} %bitcast.15, bf16[384,256]{1,0:T(8,128)(2,1)} %gate_c.3, ...), custom_call_target="tpu_custom_call" | custom-call | flops 12884901888 | bytes 157286400 | tf_op jit(solution)/shard_map/experts/pallas_call | solution.py:830
  124.7 35.6 %tail.1 = (f32[256,256]{1,0:T(8,128)}, bf16[384,256]{1,0:T(8,128)(2,1)}, bf16[384,256]{1,0:T(8,128)(2,1)}, bf16[384,256]{1,0:T(8,128)(2,1)}) custom-call(bf16[384,2048]{1,0:T(8,128)(2,1)} %get-tuple-element.28.resid_grad.refs_3_, f32[16,256]{1,0:T(8,128)} %get-tuple-element.29.earlier, bf16[2048,256]{1,0:T(8,128)(2,1)} %out_mat.1, bf16[384,256]{1,0:T(8,128)(2,1)} %gate_b.1, ...), custom_call_target="tpu_custom_call" | custom-call | tf_op jit(solution)/shard_map/tail/pallas_call | solution.py:1099
  160.4 6.6 %hand_over.1 = (f32[2048,256]{1,0:T(8,128)}, f32[2048,256]{1,0:T(8,128)}, f32[256,2048]{1,0:T(8,128)}, bf16[384,2048]{1,0:T(8,128)(2,1)}, f32[256,256]{1,0:T(8,1...) custom-call(f32[2048,256]{1,0:T(8,128)} %get-tuple-element.25.refs_0_, ...), custom_call_target="tpu_custom_call" | custom-call | tf_op jit(solution)/shard_map/hand_over/pallas_call | solution.py:1155

commit v5 on v4

--- a/solution.py
+++ b/solution.py
@@ -638,19 +638,20 @@
         take_narrow(level, 1)
         take_narrow(level, 0)
         take_wide(level, 1)
+        move_early(level, 0)
         share_level(level - 1)
-        move_early(level, 0)
         work_level(level - 1, False)
         take_wide(level, 0)
         move_early(level + 1, 1)
         work_level(level, True)
         receive_level(level, 1)
 
+        receive_level(level, 0)
+
         @pl.when(level < depth)
         def _():
             total_level(level - 1)
 
-        receive_level(level, 0)
         return carry
 
     lax.fori_loop(0, depth + 1, advance, 0)
@@ -1148,7 +1149,7 @@
 
 
 def hand_over(*arrays):
-    parts = 2
+    parts = 4
     count = len(arrays)
     anywhere = pl.BlockSpec(memory_space=pl.ANY)
     dma = pltpu.SemaphoreType.DMA((count, parts))

time: 169 us -> 170 us (level)
  no operation moved by 1% of the time
where the time goes in v5:
time: 170 us; the launch traced here: 168 us
  Pallas kernels  167 us (98%)
    pallas_call x1, Pallas kernels, experts(): pl.pallas_call(functools.partial(expert_kernel, groups, width, lanes), ou...  125 us
    pallas_call x1, Pallas kernels, tail(): pl.pallas_call(functools.partial(tail_kernel, groups, width, lanes, piece...  35.3 us
    pallas_call x1, Pallas kernels, hand_over(): pl.pallas_call(functools.partial(hand_kernel, count, parts), out_shape=tu...  6.86 us

profile of v5, /device:TPU:12, one launch (start us, length us, event | category | flops | bytes accessed | tf_op | source)
XLA Modules:
  0.0 167.8 jit_solution(17276670489535564369)
XLA Ops:
  0.6 124.9 %experts.1 = (bf16[384,2048]{1,0:T(8,128)(2,1)}, f32[16,256]{1,0:T(8,128)}, f32[2048,256]{1,0:T(8,128)}, f32[2048,256]{1,0:T(8,128)}, f32[256,2048]{1,0:T(8,128)}) custom-call(bf16[384,2048]{1,0:T(8,128)(2,1)} %resid.1, bf16[384,2048]{1,0:T(8,128)(2,1)} %cots.1, f32[1,2048]{1,0:T(1,128)} %bitcast.15, bf16[384,256]{1,0:T(8,128)(2,1)} %gate_c.3, ...), custom_call_target="tpu_custom_call" | custom-call | flops 12884901888 | bytes 157286400 | tf_op jit(solution)/shard_map/experts/pallas_call | solution.py:831
  125.6 35.3 %tail.1 = (f32[256,256]{1,0:T(8,128)}, bf16[384,256]{1,0:T(8,128)(2,1)}, bf16[384,256]{1,0:T(8,128)(2,1)}, bf16[384,256]{1,0:T(8,128)(2,1)}) custom-call(bf16[384,2048]{1,0:T(8,128)(2,1)} %get-tuple-element.28.resid_grad.refs_3_, f32[16,256]{1,0:T(8,128)} %get-tuple-element.29.earlier, bf16[2048,256]{1,0:T(8,128)(2,1)} %out_mat.1, bf16[384,256]{1,0:T(8,128)(2,1)} %gate_b.1, ...), custom_call_target="tpu_custom_call" | custom-call | tf_op jit(solution)/shard_map/tail/pallas_call | solution.py:1100
  160.9 6.9 %hand_over.1 = (f32[2048,256]{1,0:T(8,128)}, f32[2048,256]{1,0:T(8,128)}, f32[256,2048]{1,0:T(8,128)}, bf16[384,2048]{1,0:T(8,128)(2,1)}, f32[256,256]{1,0:T(8,1...) custom-call(f32[2048,256]{1,0:T(8,128)} %get-tuple-element.25.refs_0_, ...), custom_call_target="tpu_custom_call" | custom-call | tf_op jit(solution)/shard_map/hand_over/pallas_call | solution.py:1156
